TPU v7x, 128 devices: a whole 4x4x4 slice. The times are simulated.
128 devices in a mesh: sp: 16 (over z, y), tp: 8 (over x, core).
Axes of the slice: x: 4, y: 4, z: 4, core: 2. Of those that a mesh axis runs over, the one named last changes fastest.
Arguments:
- resid: bfloat16 [12288, 2048], P(('sp', 'tp')), may hold values from -6 to 6
- query_small: bfloat16 [12288, 768], P('sp', 'tp'), may hold values from -480 to 480
- query_large: bfloat16 [12288, 1280], P('sp', 'tp'), may hold values from -480 to 480
- kv_latent: bfloat16 [12288, 256], P('sp'), may hold values from -6 to 6
- rope_key: bfloat16 [12288, 32], P('sp'), may hold values from -6 to 6
- kv_gain: bfloat16 [256], replicated, may hold values from 0.099609375 to 1.8984375
- up_key_small: bfloat16 [256, 512], P(None, 'tp'), may hold values from -0.375 to 0.375
- up_value_small: bfloat16 [256, 512], P(None, 'tp'), may hold values from -0.375 to 0.375
- up_key_large: bfloat16 [256, 1024], P(None, 'tp'), may hold values from -0.375 to 0.375
- up_value_large: bfloat16 [256, 1024], P(None, 'tp'), may hold values from -0.375 to 0.375
- out_weight: bfloat16 [1536, 2048], replicated, may hold values from -0.359375 to 0.359375
- mix_gain: bfloat16 [2048], replicated, may hold values from 0.099609375 to 1.8984375
- gate_weight: bfloat16 [2048, 5632], P('sp', 'tp'), may hold values from -0.125 to 0.125
- up_weight: bfloat16 [2048, 5632], P('sp', 'tp'), may hold values from -0.125 to 0.125
- down_weight: bfloat16 [2048, 5632], P('sp', 'tp'), may hold values from -0.078125 to 0.078125
Outputs:
- layer_output: bfloat16 [12288, 2048], P(('sp', 'tp'))
All inputs are finite; a program needn't handle non-finite values.
Results may differ from a plain program's by a relative error of at most 0.014.
The roundings to bfloat16 on the way count: a program that leaves them out, or rounds other values in their place, can miss the bound.
Values may be sent and summed in bfloat16 or wider, within the bound.
A program may use at most 128 MiB of HBM per device.

v0:
```python
import math

import jax
import jax.numpy as jnp
from jax import lax
from jax.sharding import PartitionSpec as P

HEADS_SMALL = 8
NOPE_SMALL = 64
NOPE_LARGE = 128
VALUE_SMALL = 64
VALUE_LARGE = 128
ROTARY = 32


THETA = 10000.0
EPSILON = 1e-06
FLOOR = -1e30


def side_by_side(arrays, axis, dim, along):
    ends, at = ([], 0)
    for a in arrays[:-1]:
        at += a.shape[along]
        ends.append(at)
    both = jnp.concatenate(arrays, axis=along)
    return tuple(jnp.split(lax.all_gather(both, axis, axis=dim, tiled=True), ends, axis=along))


def split_up(array, dim, peers):
    shape = array.shape
    tiles = array.reshape(*shape[:dim], peers, shape[dim] // peers, *shape[dim + 1 :])
    return jnp.moveaxis(tiles, dim, 0)


def summed_on_arrival(array, axis, dim):
    tiles = split_up(array, dim, lax.axis_size(axis))
    arrived = lax.all_to_all(tiles, axis, split_axis=0, concat_axis=0, tiled=True)
    return arrived.astype(jnp.float32).sum(axis=0)


def angles(positions, width):
    inverse = THETA ** (-jnp.arange(0, width, 2).astype(jnp.float32) / width)
    phase = positions.astype(jnp.float32)[:, None] * inverse[None, :]
    return (jnp.cos(phase), jnp.sin(phase))


def rotate(values, angle_cos, angle_sin):
    half = values.shape[-1] // 2
    first = values[..., :half].astype(jnp.float32)
    second = values[..., half:].astype(jnp.float32)
    turned = jnp.concatenate(
        [first * angle_cos - second * angle_sin, second * angle_cos + first * angle_sin], axis=-1
    )
    return turned.astype(jnp.bfloat16)


def norm_rows(values, gain):
    wide = values.astype(jnp.float32)
    scaled = wide * lax.rsqrt(jnp.mean(wide * wide, axis=-1, keepdims=True) + EPSILON)
    return (scaled * gain.astype(jnp.float32)).astype(jnp.bfloat16)


def split_query(query, heads, nope, angle_cos, angle_sin):
    shaped = query.reshape(query.shape[0], heads, -1)
    return (
        shaped[..., :nope],
        rotate(shaped[..., nope:], angle_cos[:, None, :], angle_sin[:, None, :]),
    )


def absorb(state, query_parts, key_nope, shared_block, values, offset, first, scale):
    query_nope, query_turned = query_parts
    scores = jnp.einsum("qhd,khd->hqk", query_nope, key_nope, preferred_element_type=jnp.float32)
    scores = scores + jnp.einsum(
        "qhd,kd->hqk", query_turned, shared_block, preferred_element_type=jnp.float32
    )
    scores = scores * scale
    query_pos = offset + jnp.arange(query_nope.shape[0], dtype=jnp.int32)
    key_pos = first + jnp.arange(key_nope.shape[0], dtype=jnp.int32)
    allowed = key_pos[None, :] <= query_pos[:, None]
    scores = jnp.where(allowed[None], scores, FLOOR)
    maximum, total, summed = state
    new_max = jnp.maximum(maximum, jnp.max(scores, axis=-1))
    weights = jnp.where(allowed[None], jnp.exp(scores - new_max[..., None]), 0.0)
    factor = jnp.exp(maximum - new_max)
    total = total * factor + jnp.sum(weights, axis=-1)
    summed = summed * factor[..., None] + jnp.einsum(
        "hqk,khd->hqd", weights.astype(jnp.bfloat16), values, preferred_element_type=jnp.float32
    )
    return (new_max, total, summed)


def finish(group_state):
    maximum, total, summed = group_state
    out = summed / total[..., None]
    return jnp.transpose(out, (1, 0, 2)).reshape(out.shape[1], -1).astype(jnp.bfloat16)


def on_device(
    resid,
    query_small,
    query_large,
    kv_latent,
    rope_key,
    kv_gain,
    up_key_small,
    up_value_small,
    up_key_large,
    up_value_large,
    out_weight,
    mix_gain,
    gate_weight,
    up_weight,
    down_weight,
):
    rows = kv_latent.shape[0]
    offset = lax.axis_index("sp") * rows
    last = offset + rows - 1
    positions = offset + jnp.arange(rows, dtype=jnp.int32)
    angle_cos, angle_sin = angles(positions, ROTARY)
    latent_normed = norm_rows(kv_latent, kv_gain)
    rotated_key = rotate(rope_key, angle_cos, angle_sin)
    heads_small = up_key_small.shape[1] // NOPE_SMALL
    heads_large = up_key_large.shape[1] // NOPE_LARGE
    small_parts = split_query(query_small, heads_small, NOPE_SMALL, angle_cos, angle_sin)
    large_parts = split_query(query_large, heads_large, NOPE_LARGE, angle_cos, angle_sin)
    scale_small = 1.0 / math.sqrt(NOPE_SMALL + ROTARY)
    scale_large = 1.0 / math.sqrt(NOPE_LARGE + ROTARY)

    def start_state(heads, width):
        return (
            jnp.full((heads, rows), FLOOR, jnp.float32),
            jnp.zeros((heads, rows), jnp.float32),
            jnp.zeros((heads, rows, width), jnp.float32),
        )

    initial = (start_state(heads_small, VALUE_SMALL), start_state(heads_large, VALUE_LARGE))

    def consume(state, keys_small, values_small, keys_large, values_large, shared_block, first):
        length = shared_block.shape[0]
        small = absorb(
            state[0],
            small_parts,
            keys_small.reshape(length, heads_small, NOPE_SMALL),
            shared_block,
            values_small.reshape(length, heads_small, VALUE_SMALL),
            offset,
            first,
            scale_small,
        )
        large = absorb(
            state[1],
            large_parts,
            keys_large.reshape(length, heads_large, NOPE_LARGE),
            shared_block,
            values_large.reshape(length, heads_large, VALUE_LARGE),
            offset,
            first,
            scale_large,
        )
        return (small, large)

    own_keys = tuple(
        (
            jnp.dot(latent_normed, matrix, preferred_element_type=jnp.float32).astype(jnp.bfloat16)
            for matrix in (up_key_small, up_value_small, up_key_large, up_value_large)
        )
    )
    pieces = side_by_side(
        (own_keys[0], own_keys[1], own_keys[2], own_keys[3], rotated_key), "sp", 0, 1
    )
    count = pieces[0].shape[0] // rows

    def step(index, inner):
        first = index * rows
        blocks = tuple((lax.dynamic_slice_in_dim(piece, index * rows, rows, 0) for piece in pieces))
        return lax.cond(
            first <= last, lambda held: consume(held, *blocks, first), lambda held: held, inner
        )

    state = lax.fori_loop(0, count, step, initial)
    attn_small = finish(state[0])
    attn_large = finish(state[1])
    border = HEADS_SMALL * VALUE_SMALL
    all_small, all_large = (
        lax.all_to_all(attn_small, "tp", split_axis=0, concat_axis=1, tiled=True),
        lax.all_to_all(attn_large, "tp", split_axis=0, concat_axis=1, tiled=True),
    )
    mixed = jnp.dot(all_small, out_weight[:border], preferred_element_type=jnp.float32)
    mixed = mixed + jnp.dot(all_large, out_weight[border:], preferred_element_type=jnp.float32)
    middle = (resid.astype(jnp.float32) + mixed).astype(jnp.bfloat16)
    mixer_in = norm_rows(middle, mix_gain)
    gate_whole, up_whole, down_whole = side_by_side(
        (gate_weight, up_weight, down_weight), "sp", 0, 1
    )
    piece = lax.all_gather(mixer_in, "tp", axis=0, tiled=True)
    gate = jnp.dot(piece, gate_whole, preferred_element_type=jnp.float32)
    upward = jnp.dot(piece, up_whole, preferred_element_type=jnp.float32)
    hidden = (jax.nn.silu(gate) * upward).astype(jnp.bfloat16)
    branch = summed_on_arrival(
        lax.dot_general(
            hidden, down_whole, (((1,), (1,)), ((), ())), preferred_element_type=jnp.float32
        ).astype(jnp.bfloat16),
        "tp",
        0,
    )
    return (middle.astype(jnp.float32) + branch).astype(jnp.bfloat16)


def solution(mesh):
    placed = (
        P(("sp", "tp"), None),
        P("sp", "tp"),
        P("sp", "tp"),
        P("sp", None),
        P("sp", None),
        P(),
        P(None, "tp"),
        P(None, "tp"),
        P(None, "tp"),
        P(None, "tp"),
        P(),
        P(),
        P("sp", "tp"),
        P("sp", "tp"),
        P("sp", "tp"),
    )
    return jax.shard_map(
        on_device, mesh=mesh, in_specs=placed, out_specs=P(("sp", "tp"), None), check_vma=False
    )
```

profile of v0, /device:TPU:97, one launch (start us, length us, event | category | flops | bytes accessed | tf_op | source)
XLA Modules:
  0.0 399.8 jit_solution(1125508676074767138)
XLA Ops:
  16.6 78.4 %all-gather.4.cloned.1.call-done = bf16[12288,416]{0,1:T(8,128)(2,1)} async-done(((bf16[768,416]{0,1:T(8,128)(2,1)}), bf16[12288,416]{0,1:T(8,128)(2,1)}) %all-gather.4.cloned.1.call-update) | async-done | bytes 10223632 | tf_op jit(solution)/shard_map/all_gather | solution.py:27
  95.0 5.0 %fusion.103 = (bf16[12288,128]{0,1:T(8,128)(2,1)S(1)}, bf16[12288,128]{0,1:T(8,128)(2,1)}) fusion(bf16[12288,416]{0,1:T(8,128)(2,1)} %all-gather.4.cloned.1.call-done), kind=kLoop, calls=%fused_computation.130 | loop fusion | bytes 12582912 | tf_op jit(solution)/shard_map/split | solution.py:27
  100.0 4.7 %copy.34 = bf16[12288,128]{1,0:T(8,128)(2,1)} copy(bf16[12288,128]{0,1:T(8,128)(2,1)} %get-tuple-element.631) | data formatting | bytes 6291456 | tf_op jit(solution)/shard_map/while | solution.py:182
  120.6 132.4 %while.23 = (s32[]{:T(128)}, f32[1,768]{1,0:T(1,128)S(1)}, f32[1,768]{1,0:T(1,128)S(1)}, f32[1,768,64]{1,2,0:T(8,128)S(1)}, f32[1,768]{1,0:T(1,128)S(1)}, /*inde...) while((s32[]{:T(128)}, f32[1,768]{1,0:T(1,128)S(1)}, ...), condition=%wide.region_8.9_spmd, body=%wide.region_1.8_spmd.sunk | while | flops 543528960 | bytes 26487296 | solution.py:182
  120.7 10.1 %conditional.2 = ((f32[1,768]{1,0:T(1,128)S(1)}, f32[1,768]{1,0:T(1,128)S(1)}, f32[1,768,64]{1,2,0:T(8,128)S(1)}, f32[1,768]{1,0:T(1,128)S(1)}, f32[1,768]{1,0:T(1,128)S(1)}, /*index=5*/f32[1,768,128]{2,1,0:T(8,128)S(1)})) conditional(s32[]{:T(128)} %convert_element_type.277, (f32[1,768]{1,0:T(1,128)S(1)}, f32[1,768]{1,0:T(1,128)S(1)}, ...), branch_computations={%region_2.0_spmd, %region_3.7_spmd} | conditional | flops 543528960 | bytes 26486906 | solution.py:178
  130.8 10.2 %conditional.2 = ((f32[1,768]{1,0:T(1,128)S(1)}, f32[1,768]{1,0:T(1,128)S(1)}, f32[1,768,64]{1,2,0:T(8,128)S(1)}, f32[1,768]{1,0:T(1,128)S(1)}, f32[1,768]{1,0:T(1,128)S(1)}, /*index=5*/f32[1,768,128]{2,1,0:T(8,128)S(1)})) conditional(s32[]{:T(128)} %convert_element_type.277, (f32[1,768]{1,0:T(1,128)S(1)}, f32[1,768]{1,0:T(1,128)S(1)}, ...), branch_computations={%region_2.0_spmd, %region_3.7_spmd} | conditional | flops 543528960 | bytes 26486906 | solution.py:178
  141.0 10.1 %conditional.2 = ((f32[1,768]{1,0:T(1,128)S(1)}, f32[1,768]{1,0:T(1,128)S(1)}, f32[1,768,64]{1,2,0:T(8,128)S(1)}, f32[1,768]{1,0:T(1,128)S(1)}, f32[1,768]{1,0:T(1,128)S(1)}, /*index=5*/f32[1,768,128]{2,1,0:T(8,128)S(1)})) conditional(s32[]{:T(128)} %convert_element_type.277, (f32[1,768]{1,0:T(1,128)S(1)}, f32[1,768]{1,0:T(1,128)S(1)}, ...), branch_computations={%region_2.0_spmd, %region_3.7_spmd} | conditional | flops 543528960 | bytes 26486906 | solution.py:178
  151.2 10.1 %conditional.2 = ((f32[1,768]{1,0:T(1,128)S(1)}, f32[1,768]{1,0:T(1,128)S(1)}, f32[1,768,64]{1,2,0:T(8,128)S(1)}, f32[1,768]{1,0:T(1,128)S(1)}, f32[1,768]{1,0:T(1,128)S(1)}, /*index=5*/f32[1,768,128]{2,1,0:T(8,128)S(1)})) conditional(s32[]{:T(128)} %convert_element_type.277, (f32[1,768]{1,0:T(1,128)S(1)}, f32[1,768]{1,0:T(1,128)S(1)}, ...), branch_computations={%region_2.0_spmd, %region_3.7_spmd} | conditional | flops 543528960 | bytes 26486906 | solution.py:178
  161.4 10.2 %conditional.2 = ((f32[1,768]{1,0:T(1,128)S(1)}, f32[1,768]{1,0:T(1,128)S(1)}, f32[1,768,64]{1,2,0:T(8,128)S(1)}, f32[1,768]{1,0:T(1,128)S(1)}, f32[1,768]{1,0:T(1,128)S(1)}, /*index=5*/f32[1,768,128]{2,1,0:T(8,128)S(1)})) conditional(s32[]{:T(128)} %convert_element_type.277, (f32[1,768]{1,0:T(1,128)S(1)}, f32[1,768]{1,0:T(1,128)S(1)}, ...), branch_computations={%region_2.0_spmd, %region_3.7_spmd} | conditional | flops 543528960 | bytes 26486906 | solution.py:178
  171.6 10.1 %conditional.2 = ((f32[1,768]{1,0:T(1,128)S(1)}, f32[1,768]{1,0:T(1,128)S(1)}, f32[1,768,64]{1,2,0:T(8,128)S(1)}, f32[1,768]{1,0:T(1,128)S(1)}, f32[1,768]{1,0:T(1,128)S(1)}, /*index=5*/f32[1,768,128]{2,1,0:T(8,128)S(1)})) conditional(s32[]{:T(128)} %convert_element_type.277, (f32[1,768]{1,0:T(1,128)S(1)}, f32[1,768]{1,0:T(1,128)S(1)}, ...), branch_computations={%region_2.0_spmd, %region_3.7_spmd} | conditional | flops 543528960 | bytes 26486906 | solution.py:178
  181.8 10.1 %conditional.2 = ((f32[1,768]{1,0:T(1,128)S(1)}, f32[1,768]{1,0:T(1,128)S(1)}, f32[1,768,64]{1,2,0:T(8,128)S(1)}, f32[1,768]{1,0:T(1,128)S(1)}, f32[1,768]{1,0:T(1,128)S(1)}, /*index=5*/f32[1,768,128]{2,1,0:T(8,128)S(1)})) conditional(s32[]{:T(128)} %convert_element_type.277, (f32[1,768]{1,0:T(1,128)S(1)}, f32[1,768]{1,0:T(1,128)S(1)}, ...), branch_computations={%region_2.0_spmd, %region_3.7_spmd} | conditional | flops 543528960 | bytes 26486906 | solution.py:178
  191.9 10.1 %conditional.2 = ((f32[1,768]{1,0:T(1,128)S(1)}, f32[1,768]{1,0:T(1,128)S(1)}, f32[1,768,64]{1,2,0:T(8,128)S(1)}, f32[1,768]{1,0:T(1,128)S(1)}, f32[1,768]{1,0:T(1,128)S(1)}, /*index=5*/f32[1,768,128]{2,1,0:T(8,128)S(1)})) conditional(s32[]{:T(128)} %convert_element_type.277, (f32[1,768]{1,0:T(1,128)S(1)}, f32[1,768]{1,0:T(1,128)S(1)}, ...), branch_computations={%region_2.0_spmd, %region_3.7_spmd} | conditional | flops 543528960 | bytes 26486906 | solution.py:178
  202.1 10.1 %conditional.2 = ((f32[1,768]{1,0:T(1,128)S(1)}, f32[1,768]{1,0:T(1,128)S(1)}, f32[1,768,64]{1,2,0:T(8,128)S(1)}, f32[1,768]{1,0:T(1,128)S(1)}, f32[1,768]{1,0:T(1,128)S(1)}, /*index=5*/f32[1,768,128]{2,1,0:T(8,128)S(1)})) conditional(s32[]{:T(128)} %convert_element_type.277, (f32[1,768]{1,0:T(1,128)S(1)}, f32[1,768]{1,0:T(1,128)S(1)}, ...), branch_computations={%region_2.0_spmd, %region_3.7_spmd} | conditional | flops 543528960 | bytes 26486906 | solution.py:178
  212.3 10.1 %conditional.2 = ((f32[1,768]{1,0:T(1,128)S(1)}, f32[1,768]{1,0:T(1,128)S(1)}, f32[1,768,64]{1,2,0:T(8,128)S(1)}, f32[1,768]{1,0:T(1,128)S(1)}, f32[1,768]{1,0:T(1,128)S(1)}, /*index=5*/f32[1,768,128]{2,1,0:T(8,128)S(1)})) conditional(s32[]{:T(128)} %convert_element_type.277, (f32[1,768]{1,0:T(1,128)S(1)}, f32[1,768]{1,0:T(1,128)S(1)}, ...), branch_computations={%region_2.0_spmd, %region_3.7_spmd} | conditional | flops 543528960 | bytes 26486906 | solution.py:178
  222.4 10.1 %conditional.2 = ((f32[1,768]{1,0:T(1,128)S(1)}, f32[1,768]{1,0:T(1,128)S(1)}, f32[1,768,64]{1,2,0:T(8,128)S(1)}, f32[1,768]{1,0:T(1,128)S(1)}, f32[1,768]{1,0:T(1,128)S(1)}, /*index=5*/f32[1,768,128]{2,1,0:T(8,128)S(1)})) conditional(s32[]{:T(128)} %convert_element_type.277, (f32[1,768]{1,0:T(1,128)S(1)}, f32[1,768]{1,0:T(1,128)S(1)}, ...), branch_computations={%region_2.0_spmd, %region_3.7_spmd} | conditional | flops 543528960 | bytes 26486906 | solution.py:178
  232.6 10.1 %conditional.2 = ((f32[1,768]{1,0:T(1,128)S(1)}, f32[1,768]{1,0:T(1,128)S(1)}, f32[1,768,64]{1,2,0:T(8,128)S(1)}, f32[1,768]{1,0:T(1,128)S(1)}, f32[1,768]{1,0:T(1,128)S(1)}, /*index=5*/f32[1,768,128]{2,1,0:T(8,128)S(1)})) conditional(s32[]{:T(128)} %convert_element_type.277, (f32[1,768]{1,0:T(1,128)S(1)}, f32[1,768]{1,0:T(1,128)S(1)}, ...), branch_computations={%region_2.0_spmd, %region_3.7_spmd} | conditional | flops 543528960 | bytes 26486906 | solution.py:178
  242.8 10.1 %conditional.2 = ((f32[1,768]{1,0:T(1,128)S(1)}, f32[1,768]{1,0:T(1,128)S(1)}, f32[1,768,64]{1,2,0:T(8,128)S(1)}, f32[1,768]{1,0:T(1,128)S(1)}, f32[1,768]{1,0:T(1,128)S(1)}, /*index=5*/f32[1,768,128]{2,1,0:T(8,128)S(1)})) conditional(s32[]{:T(128)} %convert_element_type.277, (f32[1,768]{1,0:T(1,128)S(1)}, f32[1,768]{1,0:T(1,128)S(1)}, ...), branch_computations={%region_2.0_spmd, %region_3.7_spmd} | conditional | flops 543528960 | bytes 26486906 | solution.py:178
  253.9 5.1 %all-to-all-start.1 = ((bf16[8,96,128]{2,1,0:T(8,128)(2,1)}), bf16[8,96,128]{2,1,0:T(8,128)(2,1)S(1)}, u32[]{:S(2)}, u32[]{:S(2)}) async-start(bf16[8,96,128]{2,1,0:T(8,128)(2,1)} %bitcast.20), calls=%async_computation.1 | async-start | bytes 393216 | tf_op jit(solution)/shard_map/all_to_all | solution.py:188
  259.9 5.0 %all-to-all-done.1 = bf16[8,96,128]{2,1,0:T(8,128)(2,1)S(1)} async-done(((bf16[8,96,128]{2,1,0:T(8,128)(2,1)}), bf16[8,96,128]{2,1,0:T(8,128)(2,1)S(1)}, u32[]{:S(2)}, u32[]{:S(2)}) %all-to-all-start.1) | async-done | bytes 196640 | tf_op jit(solution)/shard_map/all_to_all | solution.py:188
  264.9 4.2 %all-to-all-start = ((bf16[8,96,64]{1,2,0:T(8,128)(2,1)}), bf16[8,96,64]{1,2,0:T(8,128)(2,1)S(1)}, u32[]{:S(2)}, u32[]{:S(2)}) async-start(bf16[8,96,64]{1,2,0:T(8,128)(2,1)} %copy.37), calls=%async_computation | async-start | bytes 262144 | tf_op jit(solution)/shard_map/all_to_all | solution.py:187
  277.6 55.9 %all-gather.6.cloned.1.call-done = bf16[768,2048]{1,0:T(8,128)(2,1)} async-done(((bf16[96,2048]{1,0:T(8,128)(2,1)}), bf16[768,2048]{1,0:T(8,128)(2,1)}) %all-gather.6.cloned.1.call-update) | async-done | bytes 3145744 | tf_op jit(solution)/shard_map/all_gather | solution.py:197
  333.5 5.2 %fusion.50 = f32[768,704]{0,1:T(8,128)S(1)} fusion(bf16[768,2048]{1,0:T(8,128)(2,1)} %all-gather.6.cloned.1.call-done, bf16[2048,2112]{0,1:T(8,128)(2,1)} %all-gather.8.cloned.1.call-done), kind=kOutput, calls=%fused_computation.61 | convolution fusion | flops 2214592512 | bytes 8192000 | tf_op jit(solution)/shard_map/dot_general | solution.py:198
  338.7 11.8 %convolution_convert_fusion = bf16[768,2048]{1,0:T(8,128)(2,1)} fusion(bf16[2048,2112]{0,1:T(8,128)(2,1)} %all-gather.8.cloned.1.call-done, f32[768,704]{0,1:T(8,128)S(1)} %fusion.50, bf16[768,2048]{1,0:T(8,128)(2,1)} %all-gather.6.cloned.1.call-done), kind=kOutput, calls=%fused_computation.57 | convolution fusion | flops 4434001920 | bytes 14221312 | tf_op jit(solution)/shard_map/dot_general | solution.py:202
  350.4 41.4 %all_to_all.37 = bf16[8,96,2048]{2,1,0:T(8,128)(2,1)S(1)} all-to-all(bf16[8,96,2048]{2,1,0:T(8,128)(2,1)} %bitcast.82), channel_id=1, replica_groups=mesh['sp'=16,'tp'=8] {'tp'}, dimensions={0} | all-to-all | bytes 6291456 | tf_op jit(solution)/shard_map/all_to_all | solution.py:38
  (264 shorter events, 167.8 us)
Async XLA Ops:
  6.5 4.8 %copy-start = (bf16[256,128]{1,0:T(8,128)(2,1)S(1)}, bf16[256,128]{1,0:T(8,128)(2,1)}, u32[]{:S(2)}) copy-start(bf16[256,128]{1,0:T(8,128)(2,1)} %param.27) | copy-start | bytes 196612
  6.5 6.2 %copy-start.4 = (bf16[768,256]{1,0:T(8,128)(2,1)S(1)}, bf16[768,256]{1,0:T(8,128)(2,1)}, u32[]{:S(2)}) copy-start(bf16[768,256]{1,0:T(8,128)(2,1)} %param.22) | copy-start | bytes 1179652
  6.5 6.2 %copy-start.13 = (bf16[256,128]{1,0:T(8,128)(2,1)S(1)}, bf16[256,128]{1,0:T(8,128)(2,1)}, u32[]{:S(2)}) copy-start(bf16[256,128]{1,0:T(8,128)(2,1)} %param.28) | copy-start | bytes 196612
  6.5 6.6 %copy-start.6 = (bf16[768,32]{0,1:T(8,128)(2,1)S(1)}, bf16[768,32]{0,1:T(8,128)(2,1)}, u32[]{:S(2)}) copy-start(bf16[768,32]{0,1:T(8,128)(2,1)} %param.23) | copy-start | bytes 147460
  6.5 8.1 %copy-start.9 = (bf16[128,704]{0,1:T(8,128)(2,1)S(1)}, bf16[128,704]{0,1:T(8,128)(2,1)}, u32[]{:S(2)}) copy-start(bf16[128,704]{0,1:T(8,128)(2,1)} %param.31) | copy-start | bytes 540676
  6.5 8.1 %copy-start.8 = (bf16[128,704]{0,1:T(8,128)(2,1)S(1)}, bf16[128,704]{0,1:T(8,128)(2,1)}, u32[]{:S(2)}) copy-start(bf16[128,704]{0,1:T(8,128)(2,1)} %param.32) | copy-start | bytes 540676
  6.6 8.1 %copy-start.7 = (bf16[128,704]{0,1:T(8,128)(2,1)S(1)}, bf16[128,704]{0,1:T(8,128)(2,1)}, u32[]{:S(2)}) copy-start(bf16[128,704]{0,1:T(8,128)(2,1)} %param.33) | copy-start | bytes 540676
  6.6 88.4 %all-gather.4.cloned.1.call-start = ((), (), s32[]{:S(2)}) async-start(), calls=%async_computation.3 | async-start | bytes 10862592 | tf_op jit(solution)/shard_map/all_gather | solution.py:27
  9.9 5.6 %copy-start.5 = (bf16[768,160]{0,1:T(8,128)(2,1)S(1)}, bf16[768,160]{0,1:T(8,128)(2,1)}, u32[]{:S(2)}) copy-start(bf16[768,160]{0,1:T(8,128)(2,1)} %param.21) | copy-start | bytes 737284
  11.3 4.4 %copy-start.10 = (bf16[768,96]{0,1:T(8,128)(2,1)S(1)}, bf16[768,96]{0,1:T(8,128)(2,1)}, u32[]{:S(2)}) copy-start(bf16[768,96]{0,1:T(8,128)(2,1)} %param.20) | copy-start | bytes 442372
  11.3 4.4 %copy-start.12 = (bf16[2048]{0:T(1024)(128)(2,1)S(1)}, bf16[2048]{0:T(1024)(128)(2,1)}, u32[]{:S(2)}) copy-start(bf16[2048]{0:T(1024)(128)(2,1)} %param.30) | copy-start | bytes 12292
  13.7 0.8 copy-start.2
  14.5 263.0 %all-gather.8.cloned.1.call-start = ((), (), s32[]{:S(2)}) async-start(), calls=%async_computation.5 | async-start | bytes 9191424 | tf_op jit(solution)/shard_map/all_gather | solution.py:27
  115.1 2.7 slice-start
  253.9 11.0 %all-to-all-start.1 = ((bf16[8,96,128]{2,1,0:T(8,128)(2,1)}), bf16[8,96,128]{2,1,0:T(8,128)(2,1)S(1)}, u32[]{:S(2)}, u32[]{:S(2)}) async-start(bf16[8,96,128]{2,1,0:T(8,128)(2,1)} %bitcast.20), calls=%async_computation.1 | async-start | bytes 393216 | tf_op jit(solution)/shard_map/all_to_all | solution.py:188
  264.9 9.5 %all-to-all-start = ((bf16[8,96,64]{1,2,0:T(8,128)(2,1)}), bf16[8,96,64]{1,2,0:T(8,128)(2,1)S(1)}, u32[]{:S(2)}, u32[]{:S(2)}) async-start(bf16[8,96,64]{1,2,0:T(8,128)(2,1)} %copy.37), calls=%async_computation | async-start | bytes 262144 | tf_op jit(solution)/shard_map/all_to_all | solution.py:187
  269.1 5.3 %copy-start.3 = (bf16[96,2048]{1,0:T(8,128)(2,1)S(1)}, bf16[96,2048]{1,0:T(8,128)(2,1)}, u32[]{:S(2)}) copy-start(bf16[96,2048]{1,0:T(8,128)(2,1)} %param.19) | copy-start | bytes 1179652
  269.1 64.3 %all-gather.6.cloned.1.call-start = ((), (), s32[]{:S(2)}) async-start(), calls=%async_computation.4 | async-start | bytes 3538944 | tf_op jit(solution)/shard_map/all_gather | solution.py:197
  272.2 4.4 %copy-start.11 = (f32[2048]{0:T(1024)S(1)}, f32[2048]{0:T(1024)}, u32[]{:S(2)}) copy-start(f32[2048]{0:T(1024)} %convert_element_type.157) | copy-start | bytes 24580
  350.4 42.8 %copy-start.1 = (bf16[256,128]{1,0:T(8,128)(2,1)S(1)}, bf16[256,128]{1,0:T(8,128)(2,1)}, u32[]{:S(2)}) copy-start(bf16[256,128]{1,0:T(8,128)(2,1)} %param.27) | copy-start | bytes 196612
Sparse Core Ops, SparseCore 0:
  14.7 80.2 all-gather.3
  97.1 76.7 all-gather.7
  277.7 55.7 all-gather.5
where the time goes:
time: 405 us; the launch traced here: 400 us
  matrix products  144 us (36%)
  waiting for transfers between devices  142 us (35%)
  blocking collectives  41.4 us (10%)
  local copies, waits for them, and re-layouts  27.6 us (7%)
  other arithmetic  20.1 us (5%)
  between operations  13.5 us (3%)
  starting transfers between devices  9.41 us (2%)
    all_gather x2, waiting for transfers between devices, side_by_side(): lax.all_gather(both, axis, axis=dim, tiled=True)  78.4 us
    all_gather x1, waiting for transfers between devices, on_device(): piece = lax.all_gather(mixer_in, 'tp', axis=0, tiled=True)  55.9 us
    dot_general x26, matrix products, absorb(): jnp.einsum('hqk,khd->hqd', weights.astype(jnp.bfloat16), values, preferre...  42.7 us
    all_to_all x1, blocking collectives, summed_on_arrival(): lax.all_to_all(tiles, axis, split_axis=0, concat_axis=0, tiled=True)  41.4 us
    dot_general x26, matrix products, absorb(): jnp.einsum('qhd,kd->hqk', query_turned, shared_block, preferred_element_t...  38.9 us
    dot_general x26, matrix products, absorb(): jnp.einsum('qhd,khd->hqk', query_nope, key_nope, preferred_element_type=j...  36 us
    while x6, local copies, waits for them, and re-layouts, on_device(): state = lax.fori_loop(0, count, step, initial)  17.2 us
    dot_general x1, matrix products, on_device(): lax.dot_general(hidden, down_whole, (((1,), (1,)), ((), ())), preferred_e...  11.8 us
  transfers between devices with their start and end apart: 5, of which 4 were waited for; matrix products, arithmetic and copies ran while one was open for 41% of the time, Pallas kernels for 0%

commit v1 on v0

v1 whole, which is shorter than its diff:
```python
import functools
import math

import jax
import jax.numpy as jnp
from jax import lax
from jax.experimental import pallas as pl
from jax.experimental.pallas import tpu as pltpu
from jax.sharding import PartitionSpec as P

NOPE_SMALL = 64
NOPE_LARGE = 128
ROTARY = 32
THETA = 10000.0
EPSILON = 1e-06
FLOOR = -1e30
ROWS = 768
LAT_ROWS = 896
D = 2048
OWN = 96
FFD = 704
QT = 256
MT = 256
F32 = jnp.float32
BF16 = jnp.bfloat16


def angles(positions, width):
    inverse = THETA ** (-jnp.arange(0, width, 2).astype(F32) / width)
    phase = positions.astype(F32)[:, None] * inverse[None, :]
    return (jnp.cos(phase), jnp.sin(phase))


def rotate(values, angle_cos, angle_sin):
    half = values.shape[-1] // 2
    first = values[..., :half].astype(F32)
    second = values[..., half:].astype(F32)
    turned = jnp.concatenate(
        [first * angle_cos - second * angle_sin, second * angle_cos + first * angle_sin], axis=-1
    )
    return turned.astype(BF16)


def norm_rows(values, gain):
    wide = values.astype(F32)
    scaled = wide * lax.rsqrt(jnp.mean(wide * wide, axis=-1, keepdims=True) + EPSILON)
    return (scaled * gain.astype(F32)).astype(BF16)


def dot(a, b, ca=1, cb=0):
    return lax.dot_general(a, b, (((ca,), (cb,)), ((), ())), preferred_element_type=F32)


class Flow:
    def __init__(self, view, size, send_sem, recv_sem, block, target):
        self.view, self.size = view, size
        self.send_sem, self.recv_sem = send_sem, recv_sem
        self.block, self.target = block, target
        self.sent = []

    def copy(self, at, lo, size, to, k):
        ref = self.view(self.block(*at), lo, size)
        return pltpu.make_async_remote_copy(
            src_ref=ref,
            dst_ref=ref,
            send_sem=self.send_sem.at[k],
            recv_sem=self.recv_sem.at[k],
            device_id=self.target(*to),
            device_id_type=pl.DeviceIdType.MESH,
        )

    def send(self, at, part, to, k):
        lo, size = self.span(part)
        self.sent.append((at, lo, size, to, k))
        self.copy(at, lo, size, to, k).start()

    def span(self, part):
        half = self.size // 2
        return {None: (0, self.size), 0: (0, half), 1: (half, half)}[part]

    def wait(self, at, part, k):
        lo, size = self.span(part)
        self.copy(at, lo, size, (1, 0), k).wait_recv()

    def finish(self):
        for at, lo, size, to, k in self.sent:
            self.copy(at, lo, size, to, k).wait_send()

    def start_u(self):
        self.send((0, 0), None, (1, 0), 0)
        self.send((0, 0), None, (-1, 0), 1)

    def spread(self, du, k):
        self.send((du, 0), None, (0, 1), k)
        self.send((du, 0), None, (0, -1), k + 1)

    def relay_v(self, du, k):
        self.wait((du, -1), None, k)
        self.send((du, -1), 0, (0, 1), k + 2)
        self.wait((du, 1), None, k + 1)
        self.send((du, 1), 1, (0, -1), k + 3)

    def end_v(self, du, k):
        self.wait((du, 2), 0, k + 2)
        self.wait((du, 2), 1, k + 3)

    def event(self, n):
        if n == 0:
            self.start_u()
            self.spread(0, 4)
        elif n == 1:
            self.wait((-1, 0), None, 0)
            self.send((-1, 0), 0, (1, 0), 2)
            self.spread(-1, 8)
        elif n == 2:
            self.wait((1, 0), None, 1)
            self.send((1, 0), 1, (-1, 0), 3)
            self.spread(1, 12)
        elif n == 3:
            self.relay_v(0, 4)
        elif n == 4:
            self.wait((2, 0), 0, 2)
            self.wait((2, 0), 1, 3)
            self.spread(2, 16)
        elif n == 5:
            self.relay_v(-1, 8)
        elif n == 6:
            self.relay_v(1, 12)
        elif n == 7:
            self.relay_v(2, 16)
        else:
            du = (0, -1, 1, 2)[n - 8]
            self.end_v(du, 4 + 4 * (n - 8))

    def line(self, n):
        if n == 0:
            self.start_u()
        elif n == 1:
            self.wait((-1, 0), None, 0)
            self.send((-1, 0), 0, (1, 0), 2)
        elif n == 2:
            self.wait((1, 0), None, 1)
            self.send((1, 0), 1, (-1, 0), 3)
        elif n == 3:
            self.wait((2, 0), 0, 2)
            self.wait((2, 0), 1, 3)


def done_at(du, dv):
    if dv == 0:
        return {0: 0, -1: 1, 1: 2, 2: 4}[du]
    if dv == 2:
        return 8 + (0, -1, 1, 2).index(du)
    return {0: 3, -1: 5, 1: 6, 2: 7}[du]


def kernel(
    lat_hbm, qs_ref, ql_ref, wk_ref, wv_ref, ow_hbm, res_hbm, gain_ref, w_hbm,
    out_ref,
    lbuf, wbuf, owbuf, mid, nbuf, obuf, abuf, ks, kl, vs, vl, ms, ml, acs, acl,
    hbuf, po, xs, xr, ra, rb, fa, fb, st, so,
    cp, la_s, la_r, lb_s, lb_r, wa_s, wa_r, wb_s, wb_r, ls_s, ls_r,
    r_s, r_r, rs_s, rs_r, o_s, o_r, os_s, os_r, d_s, d_r, f_s, f_r,
):
    sp, tp = lax.axis_index("sp"), lax.axis_index("tp")
    z, y = sp // 4, lax.rem(sp, 4)
    x, core = tp // 2, lax.rem(tp, 2)
    mesh_id = pl.DeviceIdType.MESH

    def at_sp(dy, dz):
        return lax.rem(z + dz + 4, 4) * 4 + lax.rem(y + dy + 4, 4)

    def at_x(dx, _=0):
        return lax.rem(x + dx + 4, 4)

    sibling = {"tp": x * 2 + 1 - core}
    near = [{"sp": at_sp(*d)} for d in ((1, 0), (-1, 0), (0, 1), (0, -1))]
    near += [{"tp": at_x(d) * 2 + core} for d in (1, -1)] + [sibling]

    local = [
        pltpu.make_async_copy(lat_hbm, lbuf.at[sp], cp.at[0]),
        pltpu.make_async_copy(res_hbm, mid.at[pl.ds(pl.multiple_of(tp * OWN, 32), OWN)], cp.at[1]),
        pltpu.make_async_copy(w_hbm, wbuf.at[pl.ds(pl.multiple_of(sp * 128, 128), 128)], cp.at[2]),
        pltpu.make_async_copy(ow_hbm, owbuf, cp.at[3]),
    ]
    for c in local:
        c.start()
    barrier = pltpu.get_barrier_semaphore()
    for n in near:
        pl.semaphore_signal(barrier, inc=1, device_id=n, device_id_type=mesh_id)
    pl.semaphore_wait(barrier, len(near))

    q_rows = LAT_ROWS // 4

    def lat_view(piece):
        def view(block, lo, size):
            base = pl.multiple_of((core * 2 + piece) * q_rows, 16)
            return lbuf.at[block, pl.ds(base + lo, size)]
        return view

    def w_view(piece):
        def view(block, lo, size):
            return wbuf.at[pl.ds(pl.multiple_of(block * 128, 128) + 64 * piece + lo, size)]
        return view

    def yz(du, dv):
        return at_sp(du, dv)

    def zy(du, dv):
        return at_sp(dv, du)

    def to_yz(du, dv):
        return {"sp": at_sp(du, dv)}

    def to_zy(du, dv):
        return {"sp": at_sp(dv, du)}

    def to_x(du, _):
        return {"tp": at_x(du) * 2 + core}

    lat_a = Flow(lat_view(0), q_rows, la_s, la_r, yz, to_yz)
    lat_b = Flow(lat_view(1), q_rows, lb_s, lb_r, zy, to_zy)
    w_a = Flow(w_view(0), 64, wa_s, wa_r, yz, to_yz)
    w_b = Flow(w_view(1), 64, wb_s, wb_r, zy, to_zy)

    def res_view(chip, lo, size, c=None):
        c = core if c is None else c
        return mid.at[pl.ds(pl.multiple_of((chip * 2 + c) * OWN, 32) + lo, size)]

    def o_view(chip, lo, size, c=None):
        c = core if c is None else c
        return obuf.at[chip * 2 + c, pl.ds(lo, size)]

    res = Flow(res_view, OWN, r_s, r_r, at_x, to_x)
    att = Flow(o_view, 1152, o_s, o_r, at_x, to_x)

    def beside(src, dst, s, r):
        return pltpu.make_async_remote_copy(
            src_ref=src, dst_ref=dst, send_sem=s, recv_sem=r, device_id=sibling, device_id_type=mesh_id
        )

    def share_lat(rel, c=None):
        base = pl.multiple_of((core if c is None else c) * (2 * q_rows), 64)
        ref = lbuf.at[at_sp(*rel), pl.ds(base, 2 * q_rows)]
        n = (rel[1] % 4) * 4 + rel[0] % 4
        return beside(ref, ref, ls_s.at[n], ls_r.at[n])

    def share_line(view, size, s, r, dx, c=None):
        ref = view(at_x(dx), 0, size, c)
        return beside(ref, ref, s.at[dx % 4], r.at[dx % 4])

    share_res = functools.partial(share_line, res_view, OWN, rs_s, rs_r)
    share_att = functools.partial(share_line, o_view, 1152, os_s, os_r)

    others = [(dy, dz) for dz in (0, 1, -1, 2) for dy in (0, 1, -1, 2) if (dy, dz) != (0, 0)]

    def lat_event(n):
        lat_a.event(n)
        lat_b.event(n)
        for rel in others:
            if max(done_at(*rel), done_at(rel[1], rel[0])) == n:
                share_lat(rel).start()

    scale_small = math.log2(math.e) / math.sqrt(NOPE_SMALL + ROTARY)
    scale_large = math.log2(math.e) / math.sqrt(NOPE_LARGE + ROTARY)

    def expand(block):
        latent = lbuf[block, 0:ROWS, :]
        keys = dot(wk_ref[...], latent, 1, 1).astype(BF16)
        ks[0:64, :] = keys[0:64]
        kl[0:128, :] = keys[64:192]
        for n in range(3):
            turned = lbuf[block, ROWS + 32 * n : ROWS + 32 * n + 32, :]
            ks[64:96, 256 * n : 256 * n + 256] = turned
            kl[128:160, 256 * n : 256 * n + 256] = turned
        values = dot(latent, wv_ref[...]).astype(BF16)
        vl[:, 0:128] = values[:, 0:128]
        vs[:, 0:64] = values[:, 128:192]

    def tile(i, diagonal):
        rows = pl.ds(pl.multiple_of(i * QT, QT), QT)
        for q, k, v, m, acc, scale in (
            (ql_ref, kl, vl, ml, acl, scale_large),
            (qs_ref, ks, vs, ms, acs, scale_small),
        ):
            s = dot(q[rows, :], k[...])
            if diagonal:
                row = lax.broadcasted_iota(jnp.int32, (QT, ROWS), 0) + i * QT
                col = lax.broadcasted_iota(jnp.int32, (QT, ROWS), 1)
                s = jnp.where(col <= row, s, FLOOR)
                new = jnp.max(s, axis=1, keepdims=True)
            else:
                old = m[rows, :]
                new = jnp.maximum(old[:, 0:1], jnp.max(s, axis=1, keepdims=True))
            p = jnp.exp2((s - new) * scale).astype(BF16)
            o = dot(p, v[...])
            if diagonal:
                acc[rows, :] = o
            else:
                acc[rows, :] = acc[rows, :] * jnp.exp2((old[:, 0:1] - new) * scale) + o
            m[rows, :] = jnp.broadcast_to(new, (QT, 128))

    def attend(block, diagonal):
        expand(block)

        def body(i, carry):
            tile(i, diagonal)
            return carry

        lax.fori_loop(0, ROWS // QT, body, 0)

    vs[:, 64:128] = jnp.ones((ROWS, 64), BF16)
    vl[:, 128:256] = jnp.ones((ROWS, 128), BF16)

    local[0].wait()
    lat_event(0)
    local[1].wait()
    res.line(0)
    share_res(0).start()
    attend(sp, True)
    for n in range(1, 12):
        lat_event(n)
        if n <= 3:
            res.line(n)
            share_res((-1, 1, 2)[n - 1]).start()
    local[2].wait()
    w_a.event(0)
    w_b.event(0)
    for rel in others:
        share_lat(rel, 1 - core).wait_recv()
    for dx in (0, -1, 1, 2):
        share_res(dx, 1 - core).wait_recv()

    when = {3: 1, 4: 2, 5: 3, 6: 4, 8: 5, 9: 6, 11: 7, 12: 8, 13: 9, 14: 10, 15: 11}

    def step(t, carry):
        for n, event in when.items():
            @pl.when(t == n)
            def _():
                w_a.event(event)
                w_b.event(event)
        block = lax.rem(z + t // 4, 4) * 4 + lax.rem(y + lax.rem(t, 4), 4)

        @pl.when(block < sp)
        def _():
            attend(block, False)
        return carry

    lax.fori_loop(1, 16, step, 0)

    mine = obuf.at[tp]
    mine[0:ROWS, :] = (acl[:, 0:128] / acl[:, 128:256]).astype(BF16)
    low, high = acs[0:384, :], acs[384:768, :]
    low = low / pltpu.roll(low, 64, 1)
    high = pltpu.roll(high, 64, 1) / high
    left = lax.broadcasted_iota(jnp.int32, (384, 128), 1) < 64
    mine[ROWS:1152, :] = jnp.where(left, low, high).astype(BF16)
    att.line(0)
    share_att(0).start()
    for n in range(1, 4):
        att.line(n)
        share_att((-1, 1, 2)[n - 1]).start()
    for dx in (0, -1, 1, 2):
        share_att(dx, 1 - core).wait_recv()
    for n in range(8):
        abuf[:, 512 + 128 * n : 640 + 128 * n] = obuf[n, 0:ROWS, :]
    for n in range(4):
        one = obuf[2 * n, ROWS:1152, :].astype(F32)
        two = obuf[2 * n + 1, ROWS:1152, :].astype(F32)
        abuf[0:384, 128 * n : 128 * n + 128] = jnp.where(left, one, pltpu.roll(two, 64, 1)).astype(BF16)
        abuf[384:768, 128 * n : 128 * n + 128] = jnp.where(left, pltpu.roll(one, 64, 1), two).astype(BF16)
    local[3].wait()
    res.finish()
    for dx in (0, -1, 1, 2):
        share_res(dx).wait_send()

    def project(i, carry):
        rows = pl.ds(pl.multiple_of(i * MT, MT), MT)
        wide = dot(abuf[rows, :], owbuf[...]) + mid[rows, :].astype(F32)
        middle = wide.astype(BF16)
        mid[rows, :] = middle
        wide = middle.astype(F32)
        scaled = wide * lax.rsqrt(jnp.mean(wide * wide, axis=-1, keepdims=True) + EPSILON)
        nbuf[rows, :] = (scaled * gain_ref[...].astype(F32)).astype(BF16)
        return carry

    lax.fori_loop(0, ROWS // MT, project, 0)

    def hidden(i, carry):
        rows = pl.ds(pl.multiple_of(i * MT, MT), MT)
        both = dot(nbuf[rows, :], wbuf[:, 0 : 2 * FFD])
        gate, upward = both[:, 0:FFD], both[:, FFD:]
        hbuf[rows, :] = (gate / (1.0 + jnp.exp(-gate)) * upward).astype(BF16)
        return carry

    lax.fori_loop(0, ROWS // MT, hidden, 0)

    def swap(n):
        return beside(xs.at[n], xr.at[n], d_s.at[n], d_r.at[n])

    def down(n, carry):
        chip = lax.rem(x + 2 + n * 3, 4)
        rows = pl.ds(pl.multiple_of(chip * 192, 64), 192)
        part = dot(hbuf[rows, :], wbuf[:, 2 * FFD : 3 * FFD], 1, 1).astype(BF16)

        @pl.when(core == 0)
        def _():
            po[n] = part[0:96]
            xs[n] = part[96:192]

        @pl.when(core == 1)
        def _():
            po[n] = part[96:192]
            xs[n] = part[0:96]
        swap(n).start()
        return carry

    lax.fori_loop(0, 4, down, 0)

    def hop(src, dst, to, k):
        return pltpu.make_async_remote_copy(
            src_ref=src, dst_ref=dst, send_sem=f_s.at[k], recv_sem=f_r.at[k],
            device_id=to_x(to, 0), device_id_type=mesh_id,
        )

    def summed(n):
        swap(n).wait_recv()
        return po[n].astype(F32) + xr[n].astype(F32)

    far = summed(0)
    st[0] = far.astype(BF16)
    hops = [
        hop(st.at[0, pl.ds(0, 48)], ra, 1, 0),
        hop(st.at[0, pl.ds(48, 48)], rb, -1, 1),
    ]
    hops[0].start()
    hops[1].start()
    ahead = summed(1)
    st[1, 48:96, :] = ahead[48:96].astype(BF16)
    hops.append(hop(st.at[1, pl.ds(48, 48)], fa.at[pl.ds(48, 48)], 1, 2))
    hops[2].start()
    behind = summed(3)
    st[2, 0:48, :] = behind[0:48].astype(BF16)
    hops.append(hop(st.at[2, pl.ds(0, 48)], fb.at[pl.ds(0, 48)], -1, 3))
    hops[3].start()
    hops[0].wait_recv()
    so[0] = (ahead[0:48] + ra[...].astype(F32)).astype(BF16)
    hops.append(hop(so.at[0], fa.at[pl.ds(0, 48)], 1, 4))
    hops[4].start()
    hops[1].wait_recv()
    so[1] = (behind[48:96] + rb[...].astype(F32)).astype(BF16)
    hops.append(hop(so.at[1], fb.at[pl.ds(48, 48)], -1, 5))
    hops[5].start()
    total = summed(2) + mid[pl.ds(pl.multiple_of(tp * OWN, 32), OWN), :].astype(F32)
    for h in hops[2:]:
        h.wait_recv()
    out_ref[...] = (total + fa[...].astype(F32) + fb[...].astype(F32)).astype(BF16)

    for flow in (lat_a, lat_b, w_a, w_b, att):
        flow.finish()
    for rel in others:
        share_lat(rel).wait_send()
    for dx in (0, -1, 1, 2):
        share_att(dx).wait_send()
    for n in range(4):
        swap(n).wait_send()
    for h in hops:
        h.wait_send()


def on_device(
    resid, query_small, query_large, kv_latent, rope_key, kv_gain, up_key_small, up_value_small,
    up_key_large, up_value_large, out_weight, mix_gain, gate_weight, up_weight, down_weight,
):
    rows = kv_latent.shape[0]
    positions = lax.axis_index("sp") * rows + jnp.arange(rows, dtype=jnp.int32)
    angle_cos, angle_sin = angles(positions, ROTARY)
    latent = norm_rows(kv_latent, kv_gain)
    turned = rotate(rope_key, angle_cos, angle_sin)
    turned = turned.reshape(3, 256, ROTARY).transpose(0, 2, 1).reshape(96, 256)
    lat = jnp.concatenate([latent, turned, jnp.zeros((32, 256), BF16)], axis=0)

    def turn(query, nope):
        return jnp.concatenate(
            [query[:, :nope], rotate(query[:, nope:], angle_cos, angle_sin)], axis=1
        )

    qs = turn(query_small, NOPE_SMALL)
    ql = turn(query_large, NOPE_LARGE)
    wk = jnp.concatenate([up_key_small, up_key_large], axis=1).T
    wv = jnp.concatenate([up_value_large, up_value_small], axis=1)
    w = jnp.concatenate([gate_weight, up_weight, down_weight], axis=1)

    vmem = pl.BlockSpec(memory_space=pltpu.VMEM)
    hbm = pl.BlockSpec(memory_space=pl.ANY)
    dma = pltpu.SemaphoreType.DMA
    return pl.pallas_call(
        kernel,
        out_shape=jax.ShapeDtypeStruct((OWN, D), BF16),
        in_specs=[hbm, vmem, vmem, vmem, vmem, hbm, hbm, vmem, hbm],
        out_specs=vmem,
        scratch_shapes=[
            pltpu.VMEM((16, LAT_ROWS, 256), BF16),
            pltpu.VMEM((D, 3 * FFD), BF16),
            pltpu.VMEM((1536, D), BF16),
            pltpu.VMEM((ROWS, D), BF16),
            pltpu.VMEM((ROWS, D), BF16),
            pltpu.VMEM((8, 1152, 128), BF16),
            pltpu.VMEM((ROWS, 1536), BF16),
            pltpu.VMEM((96, ROWS), BF16),
            pltpu.VMEM((160, ROWS), BF16),
            pltpu.VMEM((ROWS, 128), BF16),
            pltpu.VMEM((ROWS, 256), BF16),
            pltpu.VMEM((ROWS, 128), F32),
            pltpu.VMEM((ROWS, 128), F32),
            pltpu.VMEM((ROWS, 128), F32),
            pltpu.VMEM((ROWS, 256), F32),
            pltpu.VMEM((ROWS, FFD), BF16),
            pltpu.VMEM((4, OWN, D), BF16),
            pltpu.VMEM((4, OWN, D), BF16),
            pltpu.VMEM((4, OWN, D), BF16),
            pltpu.VMEM((48, D), BF16),
            pltpu.VMEM((48, D), BF16),
            pltpu.VMEM((OWN, D), BF16),
            pltpu.VMEM((OWN, D), BF16),
            pltpu.VMEM((3, OWN, D), BF16),
            pltpu.VMEM((2, 48, D), BF16),
            dma((4,)),
            *[dma((20,)) for _ in range(8)],
            dma((16,)), dma((16,)),
            *[dma((4,)) for _ in range(8)],
            dma((4,)), dma((4,)), dma((6,)), dma((6,)),
        ],
        compiler_params=pltpu.CompilerParams(
            collective_id=0, has_side_effects=True, vmem_limit_bytes=67043328
        ),
    )(lat, qs, ql, wk, wv, out_weight, resid, mix_gain.reshape(1, D), w)


def solution(mesh):
    placed = (
        P(("sp", "tp"), None), P("sp", "tp"), P("sp", "tp"), P("sp", None), P("sp", None), P(),
        P(None, "tp"), P(None, "tp"), P(None, "tp"), P(None, "tp"), P(), P(),
        P("sp", "tp"), P("sp", "tp"), P("sp", "tp"),
    )
    return jax.shard_map(
        on_device, mesh=mesh, in_specs=placed, out_specs=P(("sp", "tp"), None), check_vma=False
    )
```

time: 405 us -> 159 us (0.39); the launches traced: 400 us -> 158 us
  matrix products: 144 us -> 0 us
  Pallas kernels: 0 us -> 142 us
  waiting for transfers between devices: 142 us -> 0 us
  blocking collectives: 41.4 us -> 0 us
  local copies, waits for them, and re-layouts: 27.6 us -> 8.26 us
  between operations: 13.5 us -> 0.23 us
  other arithmetic: 20.1 us -> 8.07 us
  starting transfers between devices: 9.41 us -> 0 us
    dot_general x86 -> x0, matrix products: 144 us -> none  [the longest x26 42.7 us: absorb(): jnp.einsum('hqk,khd->hqd', weights.astype(jnp.bfloat16), values, preferre...]
    pallas_call x0 -> x1, Pallas kernels: none -> 142 us  [on_device(): pl.pallas_call(kernel, out_shape=jax.ShapeDtypeStruct((OWN, D), BF16), in...]
    all_gather x3 -> x0, waiting for transfers between devices: 134 us -> none  [the longest x2 78.4 us: side_by_side(): lax.all_gather(both, axis, axis=dim, tiled=True)]
    all_to_all x1 -> x0, blocking collectives: 41.4 us -> none  [summed_on_arrival(): lax.all_to_all(tiles, axis, split_axis=0, concat_axis=0, tiled=True)]
    while x6 -> x0, local copies, waits for them, and re-layouts: 17.2 us -> none  [on_device(): state = lax.fori_loop(0, count, step, initial)]
    reduce_sum x14 -> x0, other arithmetic: 12.1 us -> none  [the longest x13 11.6 us: absorb(): total = total * factor + jnp.sum(weights, axis=-1)]
    all_to_all x2 -> x0, starting transfers between devices: 9.33 us -> none  [the longest x1 5.11 us: on_device(): lax.all_to_all(attn_large, 'tp', split_axis=0, concat_axis=1, tiled=True)]
    split x4 -> x0, local copies, waits for them, and re-layouts: 8.48 us -> none  [side_by_side(): jnp.split(lax.all_gather(both, axis, axis=dim, tiled=True), ends, axis=al...]
  transfers between devices with their start and end apart: 5 -> 0, of which waited for: 4 -> 0; matrix products, arithmetic and copies ran while one was open for 41% -> 0% of each run, Pallas kernels for 0% -> 0%
where the time goes in v1:
time: 159 us; the launch traced here: 158 us
  Pallas kernels  142 us (89%)
  local copies, waits for them, and re-layouts  8.26 us (5%)
  other arithmetic  8.07 us (5%)
    pallas_call x1, Pallas kernels, on_device(): pl.pallas_call(kernel, out_shape=jax.ShapeDtypeStruct((OWN, D), BF16), in...  142 us

profile of v1, /device:TPU:97, one launch (start us, length us, event | category | flops | bytes accessed | tf_op | source)
XLA Modules:
  0.0 158.2 jit_solution(12553140092555556788)
XLA Ops:
  0.0 0.8 fusion.29
  0.9 0.2 copy.45
  1.1 0.2 copy.46
  1.2 0.8 fusion.28
  2.0 0.2 copy.51
  2.2 0.2 copy.52
  2.3 0.8 fusion.27
  3.1 0.2 copy.54
  3.3 0.2 copy.55
  3.5 2.1 %fusion.24 = (bf16[768,16]{1,0:T(8,128)(2,1)S(1)}, bf16[768,16]{1,0:T(8,128)(2,1)S(1)}, bf16[768,16]{1,0:T(8,128)(2,1)S(1)}, bf16[768,16]{1,0:T(8,128)(2,1)S(1)}...) fusion(bf16[768,16]{1,0:T(8,128)(2,1)S(1)} %copy.55, bf16[768,16]{1,0:T(8,128)(2,1)S(1)} %copy.54, ...), kind=kLoop, calls=%fused_computation.29 | loop fusion | flops 368640 | bytes 322624 | tf_op jit(solution)/shard_map/convert
  5.6 1.0 slice.35
  6.5 0.2 copy.62
  6.7 0.9 pad_maximum_fusion.ql_ref
  7.6 0.2 copy.61
  7.8 0.9 pad_maximum_fusion.1.qs_ref
  8.9 0.2 fusion
  9.1 0.2 fusion.2
  9.4 0.9 maximum_maximum_fusion.lat_hbm
  10.8 1.1 concatenate.41.w_hbm
  12.0 0.7 pad_maximum_fusion.2.wv_ref
  12.8 1.4 maximum_bitcast_fusion.wk_ref
  14.2 0.6 reshape.34.gain_ref
  14.8 141.6 %shard_map.145 = bf16[96,2048]{1,0:T(8,128)(2,1)} custom-call(bf16[896,256]{1,0:T(8,128)(2,1)} %maximum_maximum_fusion.lat_hbm, bf16[768,96]{1,0:T(8,128)(2,1)} %pad_maximum_fusion.1.qs_ref, bf16[768,160]{1,0:T(8,128)(2,1)} %pad_maximum_fusion.ql_ref, bf16[192,256]{1,0:T(8,128)(2,1)} %maximum_bitcast_fusion.wk_ref, ...), custom_call_target="tpu_custom_call" | custom-call | tf_op jit(solution)/shard_map/pallas_call | solution.py:497
  156.4 1.8 %copy.64 = bf16[96,2048]{1,0:T(8,128)(2,1)} copy(bf16[96,2048]{1,0:T(8,128)(2,1)} %shard_map.145) | data formatting | bytes 786432
  (34 shorter events, 1.0 us)
Async XLA Ops:
  0.0 7.6 %slice-start = ((bf16[768,96]{0,1:T(8,128)(2,1)}), bf16[768,64]{0,1:T(8,128)(2,1)S(1)}, s32[]{:S(2)}) async-start(bf16[768,96]{0,1:T(8,128)(2,1)} %param.16), calls=%async_computation | async-start | bytes 196608 | tf_op jit(solution)/shard_map/slice | solution.py:485
  0.0 8.9 %copy-start = (bf16[768,256]{1,0:T(8,128)(2,1)S(1)}, bf16[768,256]{1,0:T(8,128)(2,1)}, u32[]{:S(2)}) copy-start(bf16[768,256]{1,0:T(8,128)(2,1)} %param.18) | copy-start | bytes 1179652
  0.0 9.1 %copy-start.8 = (bf16[256]{0:T(256)(128)(2,1)S(1)}, bf16[256]{0:T(256)(128)(2,1)}, u32[]{:S(2)}) copy-start(bf16[256]{0:T(256)(128)(2,1)} %param.20) | copy-start | bytes 1540
  0.0 10.3 %copy-start.1 = (bf16[128,704]{0,1:T(8,128)(2,1)S(1)}, bf16[128,704]{0,1:T(8,128)(2,1)}, u32[]{:S(2)}) copy-start(bf16[128,704]{0,1:T(8,128)(2,1)} %param.27) | copy-start | bytes 540676
  0.0 10.5 %copy-start.2 = (bf16[128,704]{0,1:T(8,128)(2,1)S(1)}, bf16[128,704]{0,1:T(8,128)(2,1)}, u32[]{:S(2)}) copy-start(bf16[128,704]{0,1:T(8,128)(2,1)} %param.28) | copy-start | bytes 540676
  0.0 11.9 %copy-start.5 = (bf16[256,128]{1,0:T(8,128)(2,1)S(1)}, bf16[256,128]{1,0:T(8,128)(2,1)}, u32[]{:S(2)}) copy-start(bf16[256,128]{1,0:T(8,128)(2,1)} %param.24) | copy-start | bytes 196612
  0.9 11.8 %copy-start.4 = (bf16[256,128]{1,0:T(8,128)(2,1)S(1)}, bf16[256,128]{1,0:T(8,128)(2,1)}, u32[]{:S(2)}) copy-start(bf16[256,128]{1,0:T(8,128)(2,1)} %param.23) | copy-start | bytes 196612
  1.0 13.1 %copy-start.7 = (bf16[2048]{0:T(1024)(128)(2,1)S(1)}, bf16[2048]{0:T(1024)(128)(2,1)}, u32[]{:S(2)}) copy-start(bf16[2048]{0:T(1024)(128)(2,1)} %param.26) | copy-start | bytes 12292
  5.5 5.1 %copy-start.3 = (bf16[128,704]{0,1:T(8,128)(2,1)S(1)}, bf16[128,704]{0,1:T(8,128)(2,1)}, u32[]{:S(2)}) copy-start(bf16[128,704]{0,1:T(8,128)(2,1)} %param.29) | copy-start | bytes 540676
  5.5 6.3 %copy-start.6 = (bf16[256,64]{0,1:T(8,128)(2,1)S(1)}, bf16[256,64]{0,1:T(8,128)(2,1)}, u32[]{:S(2)}) copy-start(bf16[256,64]{0,1:T(8,128)(2,1)} %param.22) | copy-start | bytes 98308

commit v2 on v1

--- a/solution.py
+++ b/solution.py
@@ -23,28 +23,6 @@
 MT = 256
 F32 = jnp.float32
 BF16 = jnp.bfloat16
-
-
-def angles(positions, width):
-    inverse = THETA ** (-jnp.arange(0, width, 2).astype(F32) / width)
-    phase = positions.astype(F32)[:, None] * inverse[None, :]
-    return (jnp.cos(phase), jnp.sin(phase))
-
-
-def rotate(values, angle_cos, angle_sin):
-    half = values.shape[-1] // 2
-    first = values[..., :half].astype(F32)
-    second = values[..., half:].astype(F32)
-    turned = jnp.concatenate(
-        [first * angle_cos - second * angle_sin, second * angle_cos + first * angle_sin], axis=-1
-    )
-    return turned.astype(BF16)
-
-
-def norm_rows(values, gain):
-    wide = values.astype(F32)
-    scaled = wide * lax.rsqrt(jnp.mean(wide * wide, axis=-1, keepdims=True) + EPSILON)
-    return (scaled * gain.astype(F32)).astype(BF16)
 
 
 def dot(a, b, ca=1, cb=0):
@@ -155,10 +133,11 @@
 
 
 def kernel(
-    lat_hbm, qs_ref, ql_ref, wk_ref, wv_ref, ow_hbm, res_hbm, gain_ref, w_hbm,
+    lat_ref, rk_ref, trig_ref, kvg_ref, qs_in, ql_in, wks_ref, wkl_ref, wvs_ref, wvl_ref,
+    ow_hbm, res_hbm, gain_ref, gate_hbm, up_hbm, down_hbm,
     out_ref,
-    lbuf, wbuf, owbuf, mid, nbuf, obuf, abuf, ks, kl, vs, vl, ms, ml, acs, acl,
-    hbuf, po, xs, xr, ra, rb, fa, fb, st, so,
+    lbuf, wbuf, owbuf, mid, nbuf, obuf, abuf, qs_ref, ql_ref, wk_ref, wv_ref, ks, kl, vs, vl,
+    ms, ml, acs, acl, hbuf, po, xs, xr, ra, rb, fa, fb, st, so,
     cp, la_s, la_r, lb_s, lb_r, wa_s, wa_r, wb_s, wb_r, ls_s, ls_r,
     r_s, r_r, rs_s, rs_r, o_s, o_r, os_s, os_r, d_s, d_r, f_s, f_r,
 ):
@@ -177,17 +156,37 @@
     near = [{"sp": at_sp(*d)} for d in ((1, 0), (-1, 0), (0, 1), (0, -1))]
     near += [{"tp": at_x(d) * 2 + core} for d in (1, -1)] + [sibling]
 
+    column = pl.ds(pl.multiple_of(sp * 128, 128), 128)
     local = [
-        pltpu.make_async_copy(lat_hbm, lbuf.at[sp], cp.at[0]),
-        pltpu.make_async_copy(res_hbm, mid.at[pl.ds(pl.multiple_of(tp * OWN, 32), OWN)], cp.at[1]),
-        pltpu.make_async_copy(w_hbm, wbuf.at[pl.ds(pl.multiple_of(sp * 128, 128), 128)], cp.at[2]),
-        pltpu.make_async_copy(ow_hbm, owbuf, cp.at[3]),
+        pltpu.make_async_copy(res_hbm, mid.at[pl.ds(pl.multiple_of(tp * OWN, 32), OWN)], cp.at[0]),
+        pltpu.make_async_copy(gate_hbm, wbuf.at[0:FFD, column], cp.at[1]),
+        pltpu.make_async_copy(up_hbm, wbuf.at[FFD : 2 * FFD, column], cp.at[2]),
+        pltpu.make_async_copy(down_hbm, wbuf.at[2 * FFD : 3 * FFD, column], cp.at[3]),
+        pltpu.make_async_copy(ow_hbm, owbuf, cp.at[4]),
     ]
     for c in local:
         c.start()
     barrier = pltpu.get_barrier_semaphore()
     for n in near:
         pl.semaphore_signal(barrier, inc=1, device_id=n, device_id_type=mesh_id)
+
+    trig_cos, trig_sin = trig_ref[0:16, :], trig_ref[16:32, :]
+
+    def turn(first, second):
+        first, second = first.astype(F32), second.astype(F32)
+        return (
+            (first * trig_cos - second * trig_sin).astype(BF16),
+            (second * trig_cos + first * trig_sin).astype(BF16),
+        )
+
+    wide = lat_ref[...].astype(F32)
+    scaled = wide * lax.rsqrt(jnp.mean(wide * wide, axis=-1, keepdims=True) + EPSILON)
+    lbuf[sp, 0:ROWS, :] = (scaled * kvg_ref[...].astype(F32)).astype(BF16)
+    one, two = turn(rk_ref[0:16, :], rk_ref[16:32, :])
+    for n in range(3):
+        lbuf[sp, ROWS + 32 * n : ROWS + 32 * n + 16, :] = one[:, 256 * n : 256 * n + 256]
+        lbuf[sp, ROWS + 32 * n + 16 : ROWS + 32 * n + 32, :] = two[:, 256 * n : 256 * n + 256]
+    lbuf[sp, ROWS + 96 : LAT_ROWS, :] = jnp.zeros((LAT_ROWS - ROWS - 96, 256), BF16)
     pl.semaphore_wait(barrier, len(near))
 
     q_rows = LAT_ROWS // 4
@@ -200,7 +199,9 @@
 
     def w_view(piece):
         def view(block, lo, size):
-            return wbuf.at[pl.ds(pl.multiple_of(block * 128, 128) + 64 * piece + lo, size)]
+            return wbuf.at[
+                pl.ds(1056 * piece + lo, size), pl.ds(pl.multiple_of(block * 128, 128), 128)
+            ]
         return view
 
     def yz(du, dv):
@@ -220,8 +221,8 @@
 
     lat_a = Flow(lat_view(0), q_rows, la_s, la_r, yz, to_yz)
     lat_b = Flow(lat_view(1), q_rows, lb_s, lb_r, zy, to_zy)
-    w_a = Flow(w_view(0), 64, wa_s, wa_r, yz, to_yz)
-    w_b = Flow(w_view(1), 64, wb_s, wb_r, zy, to_zy)
+    w_a = Flow(w_view(0), 1056, wa_s, wa_r, yz, to_yz)
+    w_b = Flow(w_view(1), 1056, wb_s, wb_r, zy, to_zy)
 
     def res_view(chip, lo, size, c=None):
         c = core if c is None else c
@@ -252,7 +253,10 @@
     share_res = functools.partial(share_line, res_view, OWN, rs_s, rs_r)
     share_att = functools.partial(share_line, o_view, 1152, os_s, os_r)
 
-    others = [(dy, dz) for dz in (0, 1, -1, 2) for dy in (0, 1, -1, 2) if (dy, dz) != (0, 0)]
+    others = [
+        (-1, 0), (1, 0), (0, -1), (0, 1), (-1, -1), (-1, 1), (1, -1), (1, 1),
+        (2, 0), (0, 2), (2, -1), (-1, 2), (2, 1), (1, 2), (2, 2),
+    ]
 
     def lat_event(n):
         lat_a.event(n)
@@ -266,80 +270,121 @@
 
     def expand(block):
         latent = lbuf[block, 0:ROWS, :]
-        keys = dot(wk_ref[...], latent, 1, 1).astype(BF16)
-        ks[0:64, :] = keys[0:64]
-        kl[0:128, :] = keys[64:192]
+        keys = dot(latent, wk_ref[...]).astype(BF16)
+        kl[:, 0:128] = keys[:, 0:128]
+        ks[:, 0:64] = keys[:, 128:192]
         for n in range(3):
             turned = lbuf[block, ROWS + 32 * n : ROWS + 32 * n + 32, :]
-            ks[64:96, 256 * n : 256 * n + 256] = turned
-            kl[128:160, 256 * n : 256 * n + 256] = turned
-        values = dot(latent, wv_ref[...]).astype(BF16)
-        vl[:, 0:128] = values[:, 0:128]
-        vs[:, 0:64] = values[:, 128:192]
-
-    def tile(i, diagonal):
-        rows = pl.ds(pl.multiple_of(i * QT, QT), QT)
-        for q, k, v, m, acc, scale in (
-            (ql_ref, kl, vl, ml, acl, scale_large),
-            (qs_ref, ks, vs, ms, acs, scale_small),
-        ):
-            s = dot(q[rows, :], k[...])
-            if diagonal:
-                row = lax.broadcasted_iota(jnp.int32, (QT, ROWS), 0) + i * QT
-                col = lax.broadcasted_iota(jnp.int32, (QT, ROWS), 1)
-                s = jnp.where(col <= row, s, FLOOR)
-                new = jnp.max(s, axis=1, keepdims=True)
-            else:
-                old = m[rows, :]
-                new = jnp.maximum(old[:, 0:1], jnp.max(s, axis=1, keepdims=True))
-            p = jnp.exp2((s - new) * scale).astype(BF16)
-            o = dot(p, v[...])
-            if diagonal:
-                acc[rows, :] = o
-            else:
-                acc[rows, :] = acc[rows, :] * jnp.exp2((old[:, 0:1] - new) * scale) + o
-            m[rows, :] = jnp.broadcast_to(new, (QT, 128))
+            turned = turned.astype(F32).T.astype(BF16)
+            ks[256 * n : 256 * n + 256, 64:96] = turned
+            kl[256 * n : 256 * n + 256, 128:160] = turned
+        values = dot(wv_ref[...], latent, 1, 1).astype(BF16)
+        vl[0:128, :] = values[0:128]
+        vs[0:64, :] = values[128:192]
+
+    heads = (
+        (ql_ref, kl, vl, ml, acl, scale_large),
+        (qs_ref, ks, vs, ms, acs, scale_small),
+    )
 
     def attend(block, diagonal):
         expand(block)
-
-        def body(i, carry):
-            tile(i, diagonal)
-            return carry
-
-        lax.fori_loop(0, ROWS // QT, body, 0)
-
-    vs[:, 64:128] = jnp.ones((ROWS, 64), BF16)
-    vl[:, 128:256] = jnp.ones((ROWS, 128), BF16)
-
+        units = [(i, h) for i in range(ROWS // QT) for h in heads]
+        scores, soft = {}, {}
+
+        def score(u):
+            i, (q, k, *_) = units[u]
+            scores[u] = dot(k[...], q[:, i * QT : i * QT + QT])
+
+        def weigh(u):
+            i, (_, _, _, m, _, scale) = units[u]
+            s, cols = scores.pop(u), slice(i * QT, i * QT + QT)
+            if diagonal:
+                row = lax.broadcasted_iota(jnp.int32, (ROWS, QT), 0)
+                col = lax.broadcasted_iota(jnp.int32, (ROWS, QT), 1) + i * QT
+                s = jnp.where(row <= col, s, FLOOR)
+                new = jnp.max(s, axis=0, keepdims=True)
+                fade = None
+            else:
+                old = m[:, cols]
+                new = jnp.maximum(old, jnp.max(s, axis=0, keepdims=True))
+                fade = jnp.exp2((old - new) * scale)
+            m[:, cols] = new
+            soft[u] = (jnp.exp2((s - new) * scale).astype(BF16), fade)
+
+        def gather(u):
+            i, (_, _, v, _, acc, _) = units[u]
+            (p, fade), cols = soft.pop(u), slice(i * QT, i * QT + QT)
+            o = dot(v[...], p)
+            acc[:, cols] = o if diagonal else acc[:, cols] * fade + o
+
+        score(0)
+        score(1)
+        for u in range(len(units)):
+            if u + 2 < len(units):
+                score(u + 2)
+            weigh(u)
+            if u > 0:
+                gather(u - 1)
+        gather(len(units) - 1)
+
+    lat_event(0)
     local[0].wait()
-    lat_event(0)
-    local[1].wait()
     res.line(0)
     share_res(0).start()
+
+    for inp, ref, nope in ((qs_in, qs_ref, NOPE_SMALL), (ql_in, ql_ref, NOPE_LARGE)):
+        ref[0:nope, :] = inp[0:nope, :]
+        one, two = turn(inp[nope : nope + 16, :], inp[nope + 16 : nope + 32, :])
+        ref[nope : nope + 16, :] = one
+        ref[nope + 16 : nope + 32, :] = two
+    wk_ref[:, 0:128] = wkl_ref[...]
+    wk_ref[:, 128:192] = wks_ref[...].astype(F32).T.astype(BF16)
+    wv_ref[0:128, :] = wvl_ref[...].astype(F32).T.astype(BF16)
+    wv_ref[128:192, :] = wvs_ref[...]
+    vs[64:80, :] = jnp.ones((16, ROWS), BF16)
+    vl[128:144, :] = jnp.ones((16, ROWS), BF16)
+
     attend(sp, True)
-    for n in range(1, 12):
+    for n in range(1, 3):
         lat_event(n)
-        if n <= 3:
-            res.line(n)
-            share_res((-1, 1, 2)[n - 1]).start()
-    local[2].wait()
-    w_a.event(0)
-    w_b.event(0)
-    for rel in others:
-        share_lat(rel, 1 - core).wait_recv()
-    for dx in (0, -1, 1, 2):
-        share_res(dx, 1 - core).wait_recv()
-
-    when = {3: 1, 4: 2, 5: 3, 6: 4, 8: 5, 9: 6, 11: 7, 12: 8, 13: 9, 14: 10, 15: 11}
+        res.line(n)
+        share_res((-1, 1)[n - 1]).start()
+    for c in local[1:4]:
+        c.wait()
+
+    def w_event(n):
+        w_a.event(n)
+        w_b.event(n)
+
+    def w_first(n):
+        for w in (w_a, w_b):
+            w.start_u() if n == 0 else w.spread(0, 4)
+
+    todo = {t: [] for t in range(1, 17)}
+    todo[1] += [(lat_event, 3), (res.line, 3), (lambda n: share_res(2).start(), 0)]
+    for t in range(2, 9):
+        todo[t].append((lat_event, t + 2))
+    todo[9].append((lat_event, 11))
+    todo[2].append((w_first, 0))
+    todo[6].append((w_first, 1))
+    for t, n in ((10, 1), (11, 2), (12, 3), (13, 4), (14, 5), (15, 6)):
+        todo[t].append((w_event, n))
+    todo[16] = [(w_event, n) for n in range(7, 12)]
+    for t, rel in enumerate(others):
+        todo[t + 1].append((lambda r: share_lat(r, 1 - core).wait_recv(), rel))
 
     def step(t, carry):
-        for n, event in when.items():
+        dy, dz = 0, 0
+        for n in range(1, 16):
+            dy = jnp.where(t == n, others[n - 1][0], dy)
+            dz = jnp.where(t == n, others[n - 1][1], dz)
+
             @pl.when(t == n)
             def _():
-                w_a.event(event)
-                w_b.event(event)
-        block = lax.rem(z + t // 4, 4) * 4 + lax.rem(y + lax.rem(t, 4), 4)
+                for what, arg in todo[n]:
+                    what(arg)
+        block = at_sp(dy, dz)
 
         @pl.when(block < sp)
         def _():
@@ -347,14 +392,15 @@
         return carry
 
     lax.fori_loop(1, 16, step, 0)
+    for dx in (0, -1, 1, 2):
+        share_res(dx, 1 - core).wait_recv()
 
     mine = obuf.at[tp]
-    mine[0:ROWS, :] = (acl[:, 0:128] / acl[:, 128:256]).astype(BF16)
-    low, high = acs[0:384, :], acs[384:768, :]
-    low = low / pltpu.roll(low, 64, 1)
-    high = pltpu.roll(high, 64, 1) / high
+    mine[0:ROWS, :] = (acl[0:128, :] / acl[128:129, :]).T.astype(BF16)
+    small = acs[0:64, :] / acs[64:65, :]
+    small = jnp.concatenate([small[:, 0:384], small[:, 384:768]], axis=0)
+    mine[ROWS:1152, :] = small.T.astype(BF16)
     left = lax.broadcasted_iota(jnp.int32, (384, 128), 1) < 64
-    mine[ROWS:1152, :] = jnp.where(left, low, high).astype(BF16)
     att.line(0)
     share_att(0).start()
     for n in range(1, 4):
@@ -369,7 +415,7 @@
         two = obuf[2 * n + 1, ROWS:1152, :].astype(F32)
         abuf[0:384, 128 * n : 128 * n + 128] = jnp.where(left, one, pltpu.roll(two, 64, 1)).astype(BF16)
         abuf[384:768, 128 * n : 128 * n + 128] = jnp.where(left, pltpu.roll(one, 64, 1), two).astype(BF16)
-    local[3].wait()
+    local[4].wait()
     res.finish()
     for dx in (0, -1, 1, 2):
         share_res(dx).wait_send()
@@ -385,12 +431,14 @@
         return carry
 
     lax.fori_loop(0, ROWS // MT, project, 0)
+    for what, arg in todo[16]:
+        what(arg)
 
     def hidden(i, carry):
         rows = pl.ds(pl.multiple_of(i * MT, MT), MT)
-        both = dot(nbuf[rows, :], wbuf[:, 0 : 2 * FFD])
-        gate, upward = both[:, 0:FFD], both[:, FFD:]
-        hbuf[rows, :] = (gate / (1.0 + jnp.exp(-gate)) * upward).astype(BF16)
+        both = dot(wbuf[0 : 2 * FFD, :], nbuf[rows, :], 1, 1)
+        gate, upward = both[0:FFD], both[FFD:]
+        hbuf[rows, :] = (gate / (1.0 + jnp.exp(-gate)) * upward).T.astype(BF16)
         return carry
 
     lax.fori_loop(0, ROWS // MT, hidden, 0)
@@ -401,7 +449,7 @@
     def down(n, carry):
         chip = lax.rem(x + 2 + n * 3, 4)
         rows = pl.ds(pl.multiple_of(chip * 192, 64), 192)
-        part = dot(hbuf[rows, :], wbuf[:, 2 * FFD : 3 * FFD], 1, 1).astype(BF16)
+        part = dot(hbuf[rows, :], wbuf[2 * FFD : 3 * FFD, :]).astype(BF16)
 
         @pl.when(core == 0)
         def _():
@@ -474,22 +522,9 @@
 ):
     rows = kv_latent.shape[0]
     positions = lax.axis_index("sp") * rows + jnp.arange(rows, dtype=jnp.int32)
-    angle_cos, angle_sin = angles(positions, ROTARY)
-    latent = norm_rows(kv_latent, kv_gain)
-    turned = rotate(rope_key, angle_cos, angle_sin)
-    turned = turned.reshape(3, 256, ROTARY).transpose(0, 2, 1).reshape(96, 256)
-    lat = jnp.concatenate([latent, turned, jnp.zeros((32, 256), BF16)], axis=0)
-
-    def turn(query, nope):
-        return jnp.concatenate(
-            [query[:, :nope], rotate(query[:, nope:], angle_cos, angle_sin)], axis=1
-        )
-
-    qs = turn(query_small, NOPE_SMALL)
-    ql = turn(query_large, NOPE_LARGE)
-    wk = jnp.concatenate([up_key_small, up_key_large], axis=1).T
-    wv = jnp.concatenate([up_value_large, up_value_small], axis=1)
-    w = jnp.concatenate([gate_weight, up_weight, down_weight], axis=1)
+    inverse = THETA ** (-jnp.arange(0, ROTARY, 2).astype(F32) / ROTARY)
+    phase = inverse[:, None] * positions.astype(F32)[None, :]
+    trig = jnp.concatenate([jnp.cos(phase), jnp.sin(phase)], axis=0)
 
     vmem = pl.BlockSpec(memory_space=pltpu.VMEM)
     hbm = pl.BlockSpec(memory_space=pl.ANY)
@@ -497,11 +532,11 @@
     return pl.pallas_call(
         kernel,
         out_shape=jax.ShapeDtypeStruct((OWN, D), BF16),
-        in_specs=[hbm, vmem, vmem, vmem, vmem, hbm, hbm, vmem, hbm],
+        in_specs=[vmem] * 10 + [hbm, hbm, vmem, hbm, hbm, hbm],
         out_specs=vmem,
         scratch_shapes=[
             pltpu.VMEM((16, LAT_ROWS, 256), BF16),
-            pltpu.VMEM((D, 3 * FFD), BF16),
+            pltpu.VMEM((3 * FFD, D), BF16),
             pltpu.VMEM((1536, D), BF16),
             pltpu.VMEM((ROWS, D), BF16),
             pltpu.VMEM((ROWS, D), BF16),
@@ -509,12 +544,16 @@
             pltpu.VMEM((ROWS, 1536), BF16),
             pltpu.VMEM((96, ROWS), BF16),
             pltpu.VMEM((160, ROWS), BF16),
-            pltpu.VMEM((ROWS, 128), BF16),
-            pltpu.VMEM((ROWS, 256), BF16),
-            pltpu.VMEM((ROWS, 128), F32),
-            pltpu.VMEM((ROWS, 128), F32),
-            pltpu.VMEM((ROWS, 128), F32),
-            pltpu.VMEM((ROWS, 256), F32),
+            pltpu.VMEM((256, 192), BF16),
+            pltpu.VMEM((192, 256), BF16),
+            pltpu.VMEM((ROWS, 96), BF16),
+            pltpu.VMEM((ROWS, 160), BF16),
+            pltpu.VMEM((80, ROWS), BF16),
+            pltpu.VMEM((144, ROWS), BF16),
+            pltpu.VMEM((1, ROWS), F32),
+            pltpu.VMEM((1, ROWS), F32),
+            pltpu.VMEM((80, ROWS), F32),
+            pltpu.VMEM((144, ROWS), F32),
             pltpu.VMEM((ROWS, FFD), BF16),
             pltpu.VMEM((4, OWN, D), BF16),
             pltpu.VMEM((4, OWN, D), BF16),
@@ -525,7 +564,7 @@
             pltpu.VMEM((OWN, D), BF16),
             pltpu.VMEM((3, OWN, D), BF16),
             pltpu.VMEM((2, 48, D), BF16),
-            dma((4,)),
+            dma((5,)),
             *[dma((20,)) for _ in range(8)],
             dma((16,)), dma((16,)),
             *[dma((4,)) for _ in range(8)],
@@ -534,7 +573,11 @@
         compiler_params=pltpu.CompilerParams(
             collective_id=0, has_side_effects=True, vmem_limit_bytes=67043328
         ),
-    )(lat, qs, ql, wk, wv, out_weight, resid, mix_gain.reshape(1, D), w)
+    )(
+        kv_latent, rope_key.T, trig, kv_gain.reshape(1, 256), query_small.T, query_large.T,
+        up_key_small.T, up_key_large, up_value_small.T, up_value_large,
+        out_weight, resid, mix_gain.reshape(1, D), gate_weight.T, up_weight.T, down_weight.T,
+    )
 
 
 def solution(mesh):

time: 159 us -> 124 us (0.78)
  Pallas kernels: 142 us -> 118 us
  other arithmetic: 8.07 us -> 0.92 us
  local copies, waits for them, and re-layouts: 8.26 us -> 4.3 us
    pallas_call x1, Pallas kernels: 142 us -> 118 us  [on_device(): pl.pallas_call(kernel, out_shape=jax.ShapeDtypeStruct((OWN, D), BF16), in...]
    slice x10 -> x0, local copies, waits for them, and re-layouts: 3.35 us -> none  [the longest x5 2.03 us: rotate(): second = values[..., half:].astype(F32)]
    concatenate x5 -> x1, other arithmetic: 3.4 us -> 0.65 us  [on_device(): trig = jnp.concatenate([jnp.cos(phase), jnp.sin(phase)], axis=0)]
    another operation x1 -> x0, other arithmetic: 2.05 us -> none
where the time goes in v2:
time: 124 us; the launch traced here: 123 us
  Pallas kernels  118 us (95%)
  local copies, waits for them, and re-layouts  4.3 us (3%)
    pallas_call x1, Pallas kernels, on_device(): pl.pallas_call(kernel, out_shape=jax.ShapeDtypeStruct((OWN, D), BF16), in...  118 us

profile of v2, /device:TPU:97, one launch (start us, length us, event | category | flops | bytes accessed | tf_op | source)
XLA Modules:
  0.0 122.8 jit_solution(7798624785769647111)
XLA Ops:
  0.0 1.3 %reshape.19.kvg_ref = bf16[1,256]{1,0:T(2,128)(2,1)} reshape(bf16[256]{0:T(256)(128)(2,1)} %param.20) | data formatting | bytes 1024 | tf_op jit(solution)/shard_map/reshape | solution.py:577
  1.3 1.3 %reshape.20.gain_ref = bf16[1,2048]{1,0:T(2,128)(2,1)} reshape(bf16[2048]{0:T(1024)(128)(2,1)} %param.26) | data formatting | bytes 8192 | tf_op jit(solution)/shard_map/reshape | solution.py:579
  2.6 0.3 multiply_cosine_fusion
  2.8 0.7 pad_maximum_fusion.trig_ref
  3.5 117.5 %shard_map.145 = bf16[96,2048]{1,0:T(8,128)(2,1)} custom-call(bf16[768,256]{1,0:T(8,128)(2,1)} %lat_ref.1, bf16[32,768]{1,0:T(8,128)(2,1)} %bitcast.13, f32[32,768]{1,0:T(8,128)} %pad_maximum_fusion.trig_ref, bf16[1,256]{1,0:T(2,128)(2,1)} %reshape.19.kvg_ref, bf16[96,768]{1,0:T(8,128)(2,1)} %bitcast.12, bf16[160,768]{1,0:T(8,128)(2,1)} %bitcast.8, ...), custom_call_target="tpu_custom_call" | custom-call | tf_op jit(solution)/shard_map/pallas_call | solution.py:532
  121.0 1.8 %copy.17 = bf16[96,2048]{1,0:T(8,128)(2,1)} copy(bf16[96,2048]{1,0:T(8,128)(2,1)} %shard_map.145) | data formatting | bytes 786432
  (2 shorter events, 0.0 us)

commit v3 on v2

--- a/solution.py
+++ b/solution.py
@@ -133,12 +133,12 @@
 
 
 def kernel(
-    lat_ref, rk_ref, trig_ref, kvg_ref, qs_in, ql_in, wks_ref, wkl_ref, wvs_ref, wvl_ref,
-    ow_hbm, res_hbm, gain_ref, gate_hbm, up_hbm, down_hbm,
+    lat_ref, rk_ref, trig_ref, gain_ref, qs_in, ql_in, wks_ref, wkl_ref, wvs_ref, wvl_ref,
+    ow_hbm, res_hbm, gate_hbm, up_hbm, down_hbm,
     out_ref,
     lbuf, wbuf, owbuf, mid, nbuf, obuf, abuf, qs_ref, ql_ref, wk_ref, wv_ref, ks, kl, vs, vl,
-    ms, ml, acs, acl, hbuf, po, xs, xr, ra, rb, fa, fb, st, so,
-    cp, la_s, la_r, lb_s, lb_r, wa_s, wa_r, wb_s, wb_r, ls_s, ls_r,
+    ms, ml, acs, acl, po, xs, xr, ra, rb, fa, fb, st, so,
+    cp, la_s, la_r, wa_s, wa_r, wb_s, wb_r, lb_s, lb_r, ls_s, ls_r,
     r_s, r_r, rs_s, rs_r, o_s, o_r, os_s, os_r, d_s, d_r, f_s, f_r,
 ):
     sp, tp = lax.axis_index("sp"), lax.axis_index("tp")
@@ -181,7 +181,7 @@
 
     wide = lat_ref[...].astype(F32)
     scaled = wide * lax.rsqrt(jnp.mean(wide * wide, axis=-1, keepdims=True) + EPSILON)
-    lbuf[sp, 0:ROWS, :] = (scaled * kvg_ref[...].astype(F32)).astype(BF16)
+    lbuf[sp, 0:ROWS, :] = (scaled * gain_ref[:, 0:256].astype(F32)).astype(BF16)
     one, two = turn(rk_ref[0:16, :], rk_ref[16:32, :])
     for n in range(3):
         lbuf[sp, ROWS + 32 * n : ROWS + 32 * n + 16, :] = one[:, 256 * n : 256 * n + 256]
@@ -191,11 +191,12 @@
 
     q_rows = LAT_ROWS // 4
 
-    def lat_view(piece):
-        def view(block, lo, size):
-            base = pl.multiple_of((core * 2 + piece) * q_rows, 16)
-            return lbuf.at[block, pl.ds(base + lo, size)]
-        return view
+    def lat_ref_of(block, far, c, lo=0, size=q_rows):
+        base = (2 * lax.rem(x + far, 2) + c) * q_rows + lo
+        return lbuf.at[block, pl.ds(pl.multiple_of(base, 16), size)]
+
+    def lat_view(block, lo, size):
+        return lat_ref_of(block, 0, core, lo, size)
 
     def w_view(piece):
         def view(block, lo, size):
@@ -219,8 +220,10 @@
     def to_x(du, _):
         return {"tp": at_x(du) * 2 + core}
 
-    lat_a = Flow(lat_view(0), q_rows, la_s, la_r, yz, to_yz)
-    lat_b = Flow(lat_view(1), q_rows, lb_s, lb_r, zy, to_zy)
+    def by_core(du, dv):
+        return at_sp(jnp.where(core == 0, du, dv), jnp.where(core == 0, dv, du))
+
+    lat = Flow(lat_view, q_rows, la_s, la_r, by_core, lambda du, dv: {"sp": by_core(du, dv)})
     w_a = Flow(w_view(0), 1056, wa_s, wa_r, yz, to_yz)
     w_b = Flow(w_view(1), 1056, wb_s, wb_r, zy, to_zy)
 
@@ -240,11 +243,30 @@
             src_ref=src, dst_ref=dst, send_sem=s, recv_sem=r, device_id=sibling, device_id_type=mesh_id
         )
 
-    def share_lat(rel, c=None):
-        base = pl.multiple_of((core if c is None else c) * (2 * q_rows), 64)
-        ref = lbuf.at[at_sp(*rel), pl.ds(base, 2 * q_rows)]
-        n = (rel[1] % 4) * 4 + rel[0] % 4
-        return beside(ref, ref, ls_s.at[n], ls_r.at[n])
+    def number(du, dv):
+        return (dv % 4) * 4 + du % 4
+
+    def number_by_core(du, dv):
+        return jnp.where(core == 0, number(du, dv), number(dv, du))
+
+    def share_lat(rel, far):
+        ref = lat_ref_of(by_core(*rel), far, core)
+        n = number_by_core(*rel)
+        return beside(ref, ref, ls_s.at[far, n], ls_r.at[far, n])
+
+    def shared_lat(rel, far):
+        ref = lat_ref_of(at_sp(*rel), far, 1 - core)
+        n = number(*rel)
+        return beside(ref, ref, ls_s.at[far, n], ls_r.at[far, n])
+
+    def cross(rel, dx, far=0):
+        half = 0 if dx == 1 else 1
+        ref = lat_ref_of(by_core(*rel), far, core, half * (q_rows // 2), q_rows // 2)
+        n = number(*rel)
+        return pltpu.make_async_remote_copy(
+            src_ref=ref, dst_ref=ref, send_sem=lb_s.at[half, n], recv_sem=lb_r.at[half, n],
+            device_id=to_x(dx, 0), device_id_type=mesh_id,
+        )
 
     def share_line(view, size, s, r, dx, c=None):
         ref = view(at_x(dx), 0, size, c)
@@ -259,11 +281,17 @@
     ]
 
     def lat_event(n):
-        lat_a.event(n)
-        lat_b.event(n)
+        lat.event(n)
         for rel in others:
-            if max(done_at(*rel), done_at(rel[1], rel[0])) == n:
-                share_lat(rel).start()
+            if done_at(*rel) == n:
+                cross(rel, 1).start()
+                cross(rel, -1).start()
+                share_lat(rel, 0).start()
+
+    def lat_crossed(rel):
+        cross(rel, 1, 1).wait_recv()
+        cross(rel, -1, 1).wait_recv()
+        share_lat(rel, 1).start()
 
     scale_small = math.log2(math.e) / math.sqrt(NOPE_SMALL + ROTARY)
     scale_large = math.log2(math.e) / math.sqrt(NOPE_LARGE + ROTARY)
@@ -330,8 +358,6 @@
 
     lat_event(0)
     local[0].wait()
-    res.line(0)
-    share_res(0).start()
 
     for inp, ref, nope in ((qs_in, qs_ref, NOPE_SMALL), (ql_in, ql_ref, NOPE_LARGE)):
         ref[0:nope, :] = inp[0:nope, :]
@@ -346,10 +372,8 @@
     vl[128:144, :] = jnp.ones((16, ROWS), BF16)
 
     attend(sp, True)
-    for n in range(1, 3):
+    for n in range(1, 4):
         lat_event(n)
-        res.line(n)
-        share_res((-1, 1)[n - 1]).start()
     for c in local[1:4]:
         c.wait()
 
@@ -361,18 +385,27 @@
         for w in (w_a, w_b):
             w.start_u() if n == 0 else w.spread(0, 4)
 
-    todo = {t: [] for t in range(1, 17)}
-    todo[1] += [(lat_event, 3), (res.line, 3), (lambda n: share_res(2).start(), 0)]
-    for t in range(2, 9):
-        todo[t].append((lat_event, t + 2))
-    todo[9].append((lat_event, 11))
-    todo[2].append((w_first, 0))
-    todo[6].append((w_first, 1))
-    for t, n in ((10, 1), (11, 2), (12, 3), (13, 4), (14, 5), (15, 6)):
+    def res_event(n):
+        res.line(n)
+        share_res((0, -1, 1, 2)[n]).start()
+
+    order = sorted(others, key=lambda rel: done_at(*rel))
+    todo = {t: [] for t in range(1, 16)}
+    todo[1] += [(lat_event, 4), (w_first, 0)]
+    todo[1] += [(lat_crossed, order[n]) for n in range(4)]
+    todo[2] += [(lat_event, 5), (lat_event, 6), (lat_crossed, order[4])]
+    todo[3] += [(lat_event, 7), (lat_event, 8), (w_first, 1), (lat_crossed, order[5]), (lat_crossed, order[6])]
+    todo[4] += [(lat_event, 9), (lat_event, 10), (lat_event, 11), (lat_crossed, order[7]), (lat_crossed, order[8])]
+    todo[5] += [(lat_crossed, order[9]), (lat_crossed, order[10])]
+    todo[6] += [(lat_crossed, order[11]), (lat_crossed, order[12]), (res_event, 0)]
+    todo[7] += [(lat_crossed, order[13]), (lat_crossed, order[14])]
+    for t, n in ((8, 1), (9, 2), (10, 3)):
+        todo[t].append((res_event, n))
+    for t, n in ((8, 1), (9, 2), (10, 3)):
         todo[t].append((w_event, n))
-    todo[16] = [(w_event, n) for n in range(7, 12)]
     for t, rel in enumerate(others):
-        todo[t + 1].append((lambda r: share_lat(r, 1 - core).wait_recv(), rel))
+        todo[t + 1].append((lambda r: shared_lat(r, 0).wait_recv(), rel))
+        todo[t + 1].append((lambda r: shared_lat(r, 1).wait_recv(), rel))
 
     def step(t, carry):
         dy, dz = 0, 0
@@ -403,9 +436,11 @@
     left = lax.broadcasted_iota(jnp.int32, (384, 128), 1) < 64
     att.line(0)
     share_att(0).start()
+    w_event(4)
     for n in range(1, 4):
         att.line(n)
         share_att((-1, 1, 2)[n - 1]).start()
+        w_event(4 + n)
     for dx in (0, -1, 1, 2):
         share_att(dx, 1 - core).wait_recv()
     for n in range(8):
@@ -421,35 +456,31 @@
         share_res(dx).wait_send()
 
     def project(i, carry):
+        for n in range(3):
+            @pl.when(i == n)
+            def _():
+                w_event(8 + n)
         rows = pl.ds(pl.multiple_of(i * MT, MT), MT)
         wide = dot(abuf[rows, :], owbuf[...]) + mid[rows, :].astype(F32)
         middle = wide.astype(BF16)
         mid[rows, :] = middle
         wide = middle.astype(F32)
         scaled = wide * lax.rsqrt(jnp.mean(wide * wide, axis=-1, keepdims=True) + EPSILON)
-        nbuf[rows, :] = (scaled * gain_ref[...].astype(F32)).astype(BF16)
+        nbuf[rows, :] = (scaled * gain_ref[:, 256:].astype(F32)).astype(BF16)
         return carry
 
     lax.fori_loop(0, ROWS // MT, project, 0)
-    for what, arg in todo[16]:
-        what(arg)
-
-    def hidden(i, carry):
-        rows = pl.ds(pl.multiple_of(i * MT, MT), MT)
-        both = dot(wbuf[0 : 2 * FFD, :], nbuf[rows, :], 1, 1)
-        gate, upward = both[0:FFD], both[FFD:]
-        hbuf[rows, :] = (gate / (1.0 + jnp.exp(-gate)) * upward).T.astype(BF16)
-        return carry
-
-    lax.fori_loop(0, ROWS // MT, hidden, 0)
+    w_event(11)
 
     def swap(n):
         return beside(xs.at[n], xr.at[n], d_s.at[n], d_r.at[n])
 
-    def down(n, carry):
-        chip = lax.rem(x + 2 + n * 3, 4)
-        rows = pl.ds(pl.multiple_of(chip * 192, 64), 192)
-        part = dot(hbuf[rows, :], wbuf[2 * FFD : 3 * FFD, :]).astype(BF16)
+    def chunk(n, dx):
+        rows = pl.ds(pl.multiple_of(at_x(dx) * 192, 64), 192)
+        gate = dot(nbuf[rows, :], wbuf[0:FFD, :], 1, 1)
+        upward = dot(nbuf[rows, :], wbuf[FFD : 2 * FFD, :], 1, 1)
+        hidden = (gate / (1.0 + jnp.exp(-gate)) * upward).astype(BF16)
+        part = dot(hidden, wbuf[2 * FFD : 3 * FFD, :]).astype(BF16)
 
         @pl.when(core == 0)
         def _():
@@ -460,10 +491,8 @@
         def _():
             po[n] = part[96:192]
             xs[n] = part[0:96]
+
         swap(n).start()
-        return carry
-
-    lax.fori_loop(0, 4, down, 0)
 
     def hop(src, dst, to, k):
         return pltpu.make_async_remote_copy(
@@ -475,39 +504,45 @@
         swap(n).wait_recv()
         return po[n].astype(F32) + xr[n].astype(F32)
 
-    far = summed(0)
-    st[0] = far.astype(BF16)
+    chunk(0, 2)
+    chunk(1, 1)
+    st[0] = summed(0).astype(BF16)
     hops = [
         hop(st.at[0, pl.ds(0, 48)], ra, 1, 0),
         hop(st.at[0, pl.ds(48, 48)], rb, -1, 1),
+        hop(st.at[1, pl.ds(48, 48)], fa.at[pl.ds(48, 48)], 1, 2),
+        hop(st.at[2, pl.ds(0, 48)], fb.at[pl.ds(0, 48)], -1, 3),
+        hop(so.at[0], fa.at[pl.ds(0, 48)], 1, 4),
+        hop(so.at[1], fb.at[pl.ds(48, 48)], -1, 5),
     ]
     hops[0].start()
     hops[1].start()
+    chunk(2, 3)
     ahead = summed(1)
     st[1, 48:96, :] = ahead[48:96].astype(BF16)
-    hops.append(hop(st.at[1, pl.ds(48, 48)], fa.at[pl.ds(48, 48)], 1, 2))
     hops[2].start()
-    behind = summed(3)
+    chunk(3, 0)
+    behind = summed(2)
     st[2, 0:48, :] = behind[0:48].astype(BF16)
-    hops.append(hop(st.at[2, pl.ds(0, 48)], fb.at[pl.ds(0, 48)], -1, 3))
     hops[3].start()
     hops[0].wait_recv()
-    so[0] = (ahead[0:48] + ra[...].astype(F32)).astype(BF16)
-    hops.append(hop(so.at[0], fa.at[pl.ds(0, 48)], 1, 4))
+    so[0] = (po[1, 0:48, :].astype(F32) + xr[1, 0:48, :].astype(F32) + ra[...].astype(F32)).astype(BF16)
     hops[4].start()
     hops[1].wait_recv()
     so[1] = (behind[48:96] + rb[...].astype(F32)).astype(BF16)
-    hops.append(hop(so.at[1], fb.at[pl.ds(48, 48)], -1, 5))
     hops[5].start()
-    total = summed(2) + mid[pl.ds(pl.multiple_of(tp * OWN, 32), OWN), :].astype(F32)
+    total = summed(3) + mid[pl.ds(pl.multiple_of(tp * OWN, 32), OWN), :].astype(F32)
     for h in hops[2:]:
         h.wait_recv()
     out_ref[...] = (total + fa[...].astype(F32) + fb[...].astype(F32)).astype(BF16)
 
-    for flow in (lat_a, lat_b, w_a, w_b, att):
+    for flow in (lat, w_a, w_b, att):
         flow.finish()
     for rel in others:
-        share_lat(rel).wait_send()
+        for far in (0, 1):
+            share_lat(rel, far).wait_send()
+        for dx in (1, -1):
+            cross(rel, dx).wait_send()
     for dx in (0, -1, 1, 2):
         share_att(dx).wait_send()
     for n in range(4):
@@ -525,6 +560,7 @@
     inverse = THETA ** (-jnp.arange(0, ROTARY, 2).astype(F32) / ROTARY)
     phase = inverse[:, None] * positions.astype(F32)[None, :]
     trig = jnp.concatenate([jnp.cos(phase), jnp.sin(phase)], axis=0)
+    gains = jnp.concatenate([kv_gain, mix_gain]).reshape(1, 256 + D)
 
     vmem = pl.BlockSpec(memory_space=pltpu.VMEM)
     hbm = pl.BlockSpec(memory_space=pl.ANY)
@@ -532,7 +568,7 @@
     return pl.pallas_call(
         kernel,
         out_shape=jax.ShapeDtypeStruct((OWN, D), BF16),
-        in_specs=[vmem] * 10 + [hbm, hbm, vmem, hbm, hbm, hbm],
+        in_specs=[vmem] * 10 + [hbm] * 5,
         out_specs=vmem,
         scratch_shapes=[
             pltpu.VMEM((16, LAT_ROWS, 256), BF16),
@@ -554,7 +590,6 @@
             pltpu.VMEM((1, ROWS), F32),
             pltpu.VMEM((80, ROWS), F32),
             pltpu.VMEM((144, ROWS), F32),
-            pltpu.VMEM((ROWS, FFD), BF16),
             pltpu.VMEM((4, OWN, D), BF16),
             pltpu.VMEM((4, OWN, D), BF16),
             pltpu.VMEM((4, OWN, D), BF16),
@@ -565,8 +600,8 @@
             pltpu.VMEM((3, OWN, D), BF16),
             pltpu.VMEM((2, 48, D), BF16),
             dma((5,)),
-            *[dma((20,)) for _ in range(8)],
-            dma((16,)), dma((16,)),
+            *[dma((20,)) for _ in range(6)],
+            *[dma((2, 16)) for _ in range(4)],
             *[dma((4,)) for _ in range(8)],
             dma((4,)), dma((4,)), dma((6,)), dma((6,)),
         ],
@@ -574,9 +609,9 @@
             collective_id=0, has_side_effects=True, vmem_limit_bytes=67043328
         ),
     )(
-        kv_latent, rope_key.T, trig, kv_gain.reshape(1, 256), query_small.T, query_large.T,
+        kv_latent, rope_key.T, trig, gains, query_small.T, query_large.T,
         up_key_small.T, up_key_large, up_value_small.T, up_value_large,
-        out_weight, resid, mix_gain.reshape(1, D), gate_weight.T, up_weight.T, down_weight.T,
+        out_weight, resid, gate_weight.T, up_weight.T, down_weight.T,
     )
 
 

time: 124 us -> 110 us (0.89)
  Pallas kernels: 118 us -> 106 us
  local copies, waits for them, and re-layouts: 4.3 us -> 2.37 us
    pallas_call x1, Pallas kernels: 118 us -> 106 us  [on_device(): pl.pallas_call(kernel, out_shape=jax.ShapeDtypeStruct((OWN, D), BF16), in...]
    reshape x2 -> x1, local copies, waits for them, and re-layouts: 2.54 us -> 0.6 us  [on_device(): gains = jnp.concatenate([kv_gain, mix_gain]).reshape(1, 256 + D)]
where the time goes in v3:
time: 110 us
  Pallas kernels  106 us (96%)
  local copies, waits for them, and re-layouts  2.37 us (2%)
  other arithmetic  1.61 us (1%)
    pallas_call x1, Pallas kernels, on_device(): pl.pallas_call(kernel, out_shape=jax.ShapeDtypeStruct((OWN, D), BF16), in...  106 us

profile of v3, /device:TPU:97, one launch (start us, length us, event | category | flops | bytes accessed | tf_op | source)
XLA Modules:
  0.0 109.8 jit_solution(6076450189627220317)
XLA Ops:
  0.0 0.7 pad_maximum_fusion.1
  0.7 0.6 reshape.16.gain_ref
  1.3 0.3 multiply_cosine_fusion
  1.6 0.7 pad_maximum_fusion.trig_ref
  2.2 105.8 %shard_map.145 = bf16[96,2048]{1,0:T(8,128)(2,1)} custom-call(bf16[768,256]{1,0:T(8,128)(2,1)} %lat_ref.1, bf16[32,768]{1,0:T(8,128)(2,1)} %bitcast.13, f32[32,768]{1,0:T(8,128)} %pad_maximum_fusion.trig_ref, bf16[1,2304]{1,0:T(2,128)(2,1)} %reshape.16.gain_ref, bf16[96,768]{1,0:T(8,128)(2,1)} %bitcast.12, bf16[160,768]{1,0:T(8,128)(2,1)} %bitcast.8, ...), custom_call_target="tpu_custom_call" | custom-call | tf_op jit(solution)/shard_map/pallas_call | solution.py:568
  108.1 1.8 %copy.17 = bf16[96,2048]{1,0:T(8,128)(2,1)} copy(bf16[96,2048]{1,0:T(8,128)(2,1)} %shard_map.145) | data formatting | bytes 786432
  (2 shorter events, 0.0 us)

commit v4 on v3

--- a/solution.py
+++ b/solution.py
@@ -399,7 +399,7 @@
     todo[5] += [(lat_crossed, order[9]), (lat_crossed, order[10])]
     todo[6] += [(lat_crossed, order[11]), (lat_crossed, order[12]), (res_event, 0)]
     todo[7] += [(lat_crossed, order[13]), (lat_crossed, order[14])]
-    for t, n in ((8, 1), (9, 2), (10, 3)):
+    for t, n in ((14, 1), (15, 2)):
         todo[t].append((res_event, n))
     for t, n in ((8, 1), (9, 2), (10, 3)):
         todo[t].append((w_event, n))
@@ -425,8 +425,6 @@
         return carry
 
     lax.fori_loop(1, 16, step, 0)
-    for dx in (0, -1, 1, 2):
-        share_res(dx, 1 - core).wait_recv()
 
     mine = obuf.at[tp]
     mine[0:ROWS, :] = (acl[0:128, :] / acl[128:129, :]).T.astype(BF16)
@@ -441,8 +439,10 @@
         att.line(n)
         share_att((-1, 1, 2)[n - 1]).start()
         w_event(4 + n)
+    res_event(3)
     for dx in (0, -1, 1, 2):
         share_att(dx, 1 - core).wait_recv()
+        share_res(dx, 1 - core).wait_recv()
     for n in range(8):
         abuf[:, 512 + 128 * n : 640 + 128 * n] = obuf[n, 0:ROWS, :]
     for n in range(4):

time: 110 us -> 104 us (0.945); the launches traced: 110 us -> 102 us
  Pallas kernels: 106 us -> 98.4 us
    pallas_call x1, Pallas kernels: 106 us -> 98.4 us  [on_device(): pl.pallas_call(kernel, out_shape=jax.ShapeDtypeStruct((OWN, D), BF16), in...]
where the time goes in v4:
time: 104 us; the launch traced here: 102 us
  Pallas kernels  98.4 us (95%)
  local copies, waits for them, and re-layouts  2.37 us (2%)
  other arithmetic  1.61 us (2%)
    pallas_call x1, Pallas kernels, on_device(): pl.pallas_call(kernel, out_shape=jax.ShapeDtypeStruct((OWN, D), BF16), in...  98.4 us

profile of v4, /device:TPU:97, one launch (start us, length us, event | category | flops | bytes accessed | tf_op | source)
XLA Modules:
  0.0 102.4 jit_solution(15358166478579204878)
XLA Ops:
  0.0 0.7 pad_maximum_fusion.1
  0.7 0.6 reshape.16.gain_ref
  1.3 0.3 multiply_cosine_fusion
  1.6 0.7 pad_maximum_fusion.trig_ref
  2.2 98.4 %shard_map.145 = bf16[96,2048]{1,0:T(8,128)(2,1)} custom-call(bf16[768,256]{1,0:T(8,128)(2,1)} %lat_ref.1, bf16[32,768]{1,0:T(8,128)(2,1)} %bitcast.13, f32[32,768]{1,0:T(8,128)} %pad_maximum_fusion.trig_ref, bf16[1,2304]{1,0:T(2,128)(2,1)} %reshape.16.gain_ref, bf16[96,768]{1,0:T(8,128)(2,1)} %bitcast.12, bf16[160,768]{1,0:T(8,128)(2,1)} %bitcast.8, ...), custom_call_target="tpu_custom_call" | custom-call | tf_op jit(solution)/shard_map/pallas_call | solution.py:568
  100.6 1.8 %copy.17 = bf16[96,2048]{1,0:T(8,128)(2,1)} copy(bf16[96,2048]{1,0:T(8,128)(2,1)} %shard_map.145) | data formatting | bytes 786432
  (2 shorter events, 0.0 us)

commit v5 on v4

--- a/solution.py
+++ b/solution.py
@@ -399,7 +399,7 @@
     todo[5] += [(lat_crossed, order[9]), (lat_crossed, order[10])]
     todo[6] += [(lat_crossed, order[11]), (lat_crossed, order[12]), (res_event, 0)]
     todo[7] += [(lat_crossed, order[13]), (lat_crossed, order[14])]
-    for t, n in ((14, 1), (15, 2)):
+    for t, n in ((12, 1), (13, 2)):
         todo[t].append((res_event, n))
     for t, n in ((8, 1), (9, 2), (10, 3)):
         todo[t].append((w_event, n))

time: 104 us -> 102 us (0.981); the launches traced: 102 us -> 102 us
  no operation moved by 1% of the time
where the time goes in v5:
time: 102 us
  Pallas kernels  97.7 us (96%)
  local copies, waits for them, and re-layouts  2.37 us (2%)
  other arithmetic  1.61 us (2%)
    pallas_call x1, Pallas kernels, on_device(): pl.pallas_call(kernel, out_shape=jax.ShapeDtypeStruct((OWN, D), BF16), in...  97.7 us

profile of v5, /device:TPU:97, one launch (start us, length us, event | category | flops | bytes accessed | tf_op | source)
XLA Modules:
  0.0 101.7 jit_solution(8617286187554834374)
XLA Ops:
  0.0 0.7 pad_maximum_fusion.1
  0.7 0.6 reshape.16.gain_ref
  1.3 0.3 multiply_cosine_fusion
  1.6 0.7 pad_maximum_fusion.trig_ref
  2.2 97.7 %shard_map.145 = bf16[96,2048]{1,0:T(8,128)(2,1)} custom-call(bf16[768,256]{1,0:T(8,128)(2,1)} %lat_ref.1, bf16[32,768]{1,0:T(8,128)(2,1)} %bitcast.13, f32[32,768]{1,0:T(8,128)} %pad_maximum_fusion.trig_ref, bf16[1,2304]{1,0:T(2,128)(2,1)} %reshape.16.gain_ref, bf16[96,768]{1,0:T(8,128)(2,1)} %bitcast.12, bf16[160,768]{1,0:T(8,128)(2,1)} %bitcast.8, ...), custom_call_target="tpu_custom_call" | custom-call | tf_op jit(solution)/shard_map/pallas_call | solution.py:568
  100.0 1.8 %copy.17 = bf16[96,2048]{1,0:T(8,128)(2,1)} copy(bf16[96,2048]{1,0:T(8,128)(2,1)} %shard_map.145) | data formatting | bytes 786432
  (2 shorter events, 0.0 us)
